TPU v7x, 128 devices: a whole 4x4x4 slice. The times are simulated.
128 devices in a mesh: fs: 16 (over z, x), tp: 8 (over y, core).
Axes of the slice: x: 4, y: 4, z: 4, core: 2. Of those that a mesh axis runs over, the one named last changes fastest.
Arguments:
- weights: float32 [2, 5632, 2048], P(None, 'fs', 'tp'), may hold values from -6 to 6
- momentum: float32 [2, 5632, 2048], P(None, 'fs', 'tp'), may hold values from -12 to 12
- gradients: float32 [2, 5632, 2048], P(None, 'fs', 'tp'), may hold values from -140 to 140
Outputs:
- new_weights: float32 [2, 5632, 2048], P(None, 'fs', 'tp')
- new_momentum: float32 [2, 5632, 2048], P(None, 'fs', 'tp')
- update: float32 [2, 5632, 2048], P(None, 'fs', 'tp')
All inputs are finite; a program needn't handle non-finite values.
Results may differ from a plain program's by a relative error of at most 0.035.
Values may be sent and summed in bfloat16 or wider, within the bound.
No kernel may reach another device: no remote copies, remote signals or barrier semaphores. Data moves between devices by JAX's collectives and lax.ppermute only.
A program may use at most 64 MiB of HBM per device.

v0:
```python
import math

import jax
import jax.numpy as jnp
from jax import lax
from jax.sharding import PartitionSpec as P

D = 2048
FF = 5632
ITERS = 3


MOMENTUM_DECAY = 0.95
FIRST_COEF = 3.4445
SECOND_COEF = -4.775
THIRD_COEF = 2.0315
LEARN_RATE = 0.02
WEIGHT_DECAY = 0.1
EPSILON = 1e-07
STEP_SCALE = 0.2
NORM_SAFETY = 1.8


def per_device(weights, momentum, gradients):
    new_momentum = MOMENTUM_DECAY * momentum + gradients
    iterate = gradients + MOMENTUM_DECAY * new_momentum
    for step in range(ITERS):
        plain = iterate.astype(jnp.bfloat16)
        row_whole = lax.all_gather(plain, "tp", axis=2, tiled=True)
        partial_value = jnp.einsum(
            "prj,prk->pjk", plain, row_whole, preferred_element_type=jnp.float32
        )
        gram_rows = lax.psum(partial_value, "fs")
        gram_bf = gram_rows.astype(jnp.bfloat16)
        if step == 0:
            squares = lax.psum(jnp.sum(gram_rows * gram_rows, axis=(1, 2)), "tp")
        if step == 0:
            ratio = (1.0 / (NORM_SAFETY * jnp.sqrt(jnp.sqrt(squares / D)) + EPSILON))[:, None, None]
        else:
            ratio = 1.0
        cubed = jnp.einsum("prk,pjk->prj", row_whole, gram_bf, preferred_element_type=jnp.float32)
        cubed = (cubed * ratio**3).astype(jnp.bfloat16)
        folded = jnp.einsum(
            "prk,pjk->prj",
            lax.all_gather(cubed, "tp", axis=2, tiled=True),
            gram_bf,
            preferred_element_type=jnp.float32,
        )
        iterate = (
            FIRST_COEF * ratio * iterate
            + SECOND_COEF * cubed.astype(jnp.float32)
            + THIRD_COEF * (ratio * ratio) * folded
        )
    update = STEP_SCALE * math.sqrt(max(FF, D)) * iterate
    new_weights = weights * (1.0 - LEARN_RATE * WEIGHT_DECAY) - LEARN_RATE * update
    return (new_weights, new_momentum, update)


def solution(mesh):
    in_specs = (P(None, "fs", "tp"), P(None, "fs", "tp"), P(None, "fs", "tp"))
    out_specs = (P(None, "fs", "tp"), P(None, "fs", "tp"), P(None, "fs", "tp"))
    return jax.shard_map(
        per_device, mesh=mesh, in_specs=in_specs, out_specs=out_specs, check_vma=False
    )
```

profile of v0, /device:TPU:1, one launch (start us, length us, event | category | flops | bytes accessed | tf_op | source)
XLA Modules:
  0.0 567.1 jit_solution(7577608020832004944)
XLA Ops:
  7.2 2.4 fusion.10
  9.7 34.2 %all-gather.7.cloned.1.call-done = bf16[2,352,2048]{2,1,0:T(8,128)(2,1)} async-done(((bf16[2,352,256]{2,1,0:T(8,128)(2,1)}), bf16[2,352,2048]{2,1,0:T(8,128)(2,1)}) %all-gather.7.cloned.1.call-update) | async-done | bytes 2883600 | tf_op jit(solution)/shard_map/all_gather | solution.py:29
  43.9 5.2 fusion.13
  49.1 0.0 all-gather.9.cloned.1.call-start
  49.2 104.0 %all-reduce.4.cloned.1.call-done = f32[2,256,2048]{2,1,0:T(8,128)} async-done(((f32[2,256,2048]{2,1,0:T(8,128)}), f32[2,256,2048]{2,1,0:T(8,128)}) %all-reduce.4.cloned.1.call-update) | async-done | bytes 4194320 | tf_op jit(solution)/shard_map/psum | solution.py:33
  153.2 2.8 multiply_reduce_fusion
  156.0 12.8 %psum.29 = f32[2]{0:T(128)S(1)} all-reduce(f32[2]{0:T(128)S(1)} %multiply_reduce_fusion), channel_id=1, replica_groups=mesh['fs'=16,'tp'=8] {'tp'}, use_global_device_ids=true, to_apply=%region_2.0 | all-reduce | flops 2 | bytes 16 | tf_op jit(solution)/shard_map/psum | solution.py:36
  168.9 3.9 fusion.3
  172.9 29.7 %all-gather.9.cloned.1.call-done = bf16[2,352,2048]{2,1,0:T(8,128)(2,1)} async-done(((bf16[2,352,256]{2,1,0:T(8,128)(2,1)}), bf16[2,352,2048]{2,1,0:T(8,128)(2,1)}) %all-gather.9.cloned.1.call-update) | async-done | bytes 2883600 | tf_op jit(solution)/shard_map/all_gather | solution.py:45
  202.6 5.2 fusion.11
  207.8 0.0 all-gather.13.cloned.1.call-start
  207.9 31.0 %all-gather.11.cloned.1.call-done = bf16[2,352,2048]{2,1,0:T(8,128)(2,1)} async-done(((bf16[2,352,256]{2,1,0:T(8,128)(2,1)}), bf16[2,352,2048]{2,1,0:T(8,128)(2,1)}) %all-gather.11.cloned.1.call-update) | async-done | bytes 2883600 | tf_op jit(solution)/shard_map/all_gather | solution.py:29
  238.9 5.2 fusion.14
  244.1 100.6 %all-reduce.5 = bf16[2,256,2048]{2,1,0:T(8,128)(2,1)S(1)} all-reduce(f32[2,256,2048]{2,1,0:T(8,128)} %fusion.14), channel_id=1, replica_groups=mesh['fs'=16,'tp'=8] {'fs'}, use_global_device_ids=true, to_apply=%region_3.0 | all-reduce | flops 1048576 | bytes 6291456 | tf_op jit(solution)/shard_map/psum | solution.py:33
  344.7 3.5 convolution_convert_fusion.1
  348.3 0.0 all-gather.15.cloned.1.call-start
  348.3 31.9 %all-gather.13.cloned.1.call-done = bf16[2,352,2048]{2,1,0:T(8,128)(2,1)} async-done(((bf16[2,352,256]{2,1,0:T(8,128)(2,1)}), bf16[2,352,2048]{2,1,0:T(8,128)(2,1)}) %all-gather.13.cloned.1.call-update) | async-done | bytes 2883600 | tf_op jit(solution)/shard_map/all_gather | solution.py:45
  380.2 3.5 fusion.12
  383.8 31.1 %all-gather.15.cloned.1.call-done = bf16[2,352,2048]{2,1,0:T(8,128)(2,1)} async-done(((bf16[2,352,256]{2,1,0:T(8,128)(2,1)}), bf16[2,352,2048]{2,1,0:T(8,128)(2,1)}) %all-gather.15.cloned.1.call-update) | async-done | bytes 2883600 | tf_op jit(solution)/shard_map/all_gather | solution.py:29
  414.9 5.2 fusion.15
  420.1 100.6 %all-reduce.6 = bf16[2,256,2048]{2,1,0:T(8,128)(2,1)S(1)} all-reduce(f32[2,256,2048]{2,1,0:T(8,128)} %fusion.15), channel_id=1, replica_groups=mesh['fs'=16,'tp'=8] {'fs'}, use_global_device_ids=true, to_apply=%region_4.0 | all-reduce | flops 1048576 | bytes 6291456 | tf_op jit(solution)/shard_map/psum | solution.py:33
  520.7 3.6 convolution_convert_fusion
  524.3 32.0 %all-gather.17.cloned.1.call-done = bf16[2,352,2048]{2,1,0:T(8,128)(2,1)} async-done(((bf16[2,352,256]{2,1,0:T(8,128)(2,1)}), bf16[2,352,2048]{2,1,0:T(8,128)(2,1)}) %all-gather.17.cloned.1.call-update) | async-done | bytes 2883600 | tf_op jit(solution)/shard_map/all_gather | solution.py:45
  556.2 4.0 broadcast_multiply_fusion
  (17 shorter events, 0.3 us)
Async XLA Ops:
  7.2 36.7 %all-gather.7.cloned.1.call-start = ((), (), s32[]{:S(2)}) async-start(), calls=%async_computation | async-start | bytes 3244032 | tf_op jit(solution)/shard_map/all_gather | solution.py:29
  9.7 143.5 %all-reduce.4.cloned.1.call-start = ((), (), s32[]{:S(2)}) async-start(), calls=%async_computation.1 | async-start | bytes 8388608 | tf_op jit(solution)/shard_map/psum | solution.py:33
  49.1 119.8 %copy-start = (bf16[2,352,2048]{2,1,0:T(8,128)(2,1)S(1)}, bf16[2,352,2048]{2,1,0:T(8,128)(2,1)}, u32[]{:S(2)}) copy-start(bf16[2,352,2048]{2,1,0:T(8,128)(2,1)} %all-gather.7.cloned.1.call-done) | copy-start | bytes 8650756
  49.1 153.4 %all-gather.9.cloned.1.call-start = ((), (), s32[]{:S(2)}) async-start(), calls=%async_computation.2 | async-start | bytes 3244032 | tf_op jit(solution)/shard_map/all_gather | solution.py:45
  172.8 66.1 %all-gather.11.cloned.1.call-start = ((), (), s32[]{:S(2)}) async-start(), calls=%async_computation.3 | async-start | bytes 3244032 | tf_op jit(solution)/shard_map/all_gather | solution.py:29
  207.8 172.4 %all-gather.13.cloned.1.call-start = ((), (), s32[]{:S(2)}) async-start(), calls=%async_computation.4 | async-start | bytes 3244032 | tf_op jit(solution)/shard_map/all_gather | solution.py:45
  348.3 66.6 %all-gather.15.cloned.1.call-start = ((), (), s32[]{:S(2)}) async-start(), calls=%async_computation.5 | async-start | bytes 3244032 | tf_op jit(solution)/shard_map/all_gather | solution.py:29
  383.8 172.5 %all-gather.17.cloned.1.call-start = ((), (), s32[]{:S(2)}) async-start(), calls=%async_computation.6 | async-start | bytes 3244032 | tf_op jit(solution)/shard_map/all_gather | solution.py:45
  520.7 35.6 %copy-start.1 = (f32[2,352,256]{2,1,0:T(8,128)S(1)}, f32[2,352,256]{2,1,0:T(8,128)}, u32[]{:S(2)}) copy-start(f32[2,352,256]{2,1,0:T(8,128)} %param.3) | copy-start | bytes 2162692
Sparse Core Ops, SparseCore 0:
  10.2 33.6 all-gather.6
  49.2 103.9 all-reduce.3
  172.9 29.5 all-gather.8
  207.9 30.9 all-gather.10
  348.4 31.7 all-gather.12
  383.9 30.9 all-gather.14
  524.4 31.8 all-gather.16
where the time goes:
time: 568 us; the launch traced here: 567 us
  waiting for transfers between devices  294 us (52%)
  blocking collectives  214 us (38%)
  matrix products  39.3 us (7%)
  between operations  14.2 us (2%)
    psum x2, blocking collectives, per_device(): gram_rows = lax.psum(partial_value, 'fs')  201 us
    psum x1, waiting for transfers between devices, per_device(): gram_rows = lax.psum(partial_value, 'fs')  104 us
    all_gather x3, waiting for transfers between devices, per_device(): row_whole = lax.all_gather(plain, 'tp', axis=2, tiled=True)  96.3 us
    all_gather x3, waiting for transfers between devices, per_device(): lax.all_gather(cubed, 'tp', axis=2, tiled=True)  93.6 us
    dot_general x3, matrix products, per_device(): jnp.einsum('prj,prk->pjk', plain, row_whole, preferred_element_type=jnp.f...  15.6 us
    psum x1, blocking collectives, per_device(): squares = lax.psum(jnp.sum(gram_rows * gram_rows, axis=(1, 2)), 'tp')  12.8 us
    dot_general x3, matrix products, per_device(): jnp.einsum('prk,pjk->prj', lax.all_gather(cubed, 'tp', axis=2, tiled=True...  12.8 us
  transfers between devices with their start and end apart: 7, of which 7 were waited for; matrix products, arithmetic and copies ran while one was open for 0% of the time, Pallas kernels for 0%

commit v1 on v0

v1 whole, which is shorter than its diff:
```python
import math

import jax
import jax.numpy as jnp
from jax import lax
from jax.sharding import Mesh, PartitionSpec as P

D = 2048
FF = 5632

MOMENTUM_DECAY = 0.95
A1 = 3.4445
A2 = -4.775
A3 = 2.0315
LEARN_RATE = 0.02
WEIGHT_DECAY = 0.1
EPSILON = 1e-07
STEP_SCALE = 0.2
NORM_SAFETY = 1.8

BF = jnp.bfloat16
F32 = jnp.float32


def gather(value, axes, count):
    spread = jnp.broadcast_to(value[None], (count,) + value.shape)
    return lax.all_to_all(spread, axes, split_axis=0, concat_axis=0, tiled=False)


def swap(value, axis):
    return lax.ppermute(value, axis, [(0, 1), (1, 0)])


def dot(left, right):
    return jnp.dot(left, right, preferred_element_type=F32)


def mul(left, right):
    return dot(left.astype(BF), right)


def mul_split(left, right):
    rows = left.shape[0]
    high = left.astype(BF)
    low = (left - high.astype(F32)).astype(BF)
    both = dot(jnp.concatenate([high, low], 0), right)
    return both[:rows] + both[rows:]


def whole_gram(rows, core):
    part = gather(rows, ("y", "z", "xh"), 32).reshape(D // 2, D)
    other = swap(part, "c")
    first = jnp.where(core == 0, part, other)
    second = jnp.where(core == 0, other, part)
    return jnp.concatenate([first, second], 0)


def per_device(weights, momentum, gradients):
    mat = lax.axis_index("xp")
    core = lax.axis_index("c")
    slot = core * 4 + lax.axis_index("y")

    new_momentum = MOMENTUM_DECAY * momentum + gradients
    iterate = gradients + MOMENTUM_DECAY * new_momentum
    plain = iterate.astype(BF)

    mine = jnp.where(mat == 0, plain[0], plain[1])
    other = jnp.where(mat == 0, plain[1], plain[0])
    block = jnp.concatenate([mine, swap(other, "xp")], 0)

    near = gather(block, "y", 4)
    far = swap(near, "c")
    rows_whole = jnp.concatenate(
        [jnp.where(core == 0, near, far), jnp.where(core == 0, far, near)], 0
    )

    partial = jnp.einsum("ki,nkj->inj", block, rows_whole, preferred_element_type=F32)
    partial = partial.astype(BF).reshape(8, 32, D)
    pieces = lax.all_to_all(partial, ("z", "xh"), split_axis=0, concat_axis=0)
    gram_rows = jnp.sum(pieces.astype(F32), axis=0).astype(BF)

    gram = whole_gram(gram_rows, core)
    squares = jnp.sum(jnp.square(gram.astype(F32)))
    ratio = 1.0 / (NORM_SAFETY * jnp.sqrt(jnp.sqrt(squares / D)) + EPSILON)
    q = ratio * ratio

    g = gram_rows.astype(F32)
    t1 = q * dot(gram_rows, gram)
    hold = q * (A1 * g + A2 * t1 + A3 * q * mul(t1, gram))
    t2 = q * mul(hold, gram)
    next_rows = A1 * hold + q * mul(A2 * hold + A3 * t2, gram)
    gram1 = whole_gram(next_rows.astype(BF), core)

    own = lax.dynamic_slice_in_dim(rows_whole, slot * 88, 88, axis=1)
    own = own.transpose(1, 0, 2).reshape(88, D)
    u = q * dot(own, gram)
    x1 = ratio * (A1 * own.astype(F32) + A2 * u + A3 * q * mul(u, gram))
    x2 = A1 * x1 + mul(A2 * x1 + A3 * mul(x1, gram1), gram1)

    def second_gram(value, product):
        v1 = product(value, gram1)
        v2 = A1 * v1 + product(A2 * v1 + A3 * product(v1, gram1), gram1)
        return A1 * v2 + product(A2 * v2 + A3 * product(v2, gram1), gram1)

    w = second_gram(x2, mul)
    x3 = A1 * x2 + second_gram(A2 * x2 + A3 * w, mul_split)

    back = x3.astype(BF).reshape(88, 8, 256).transpose(1, 0, 2)
    back = lax.all_to_all(back, ("c", "y"), split_axis=0, concat_axis=0).reshape(704, 256)
    kept = back[:352]
    came = swap(back[352:], "xp")
    both = jnp.stack([jnp.where(mat == 0, kept, came), jnp.where(mat == 0, came, kept)])

    update = STEP_SCALE * math.sqrt(max(FF, D)) * both.astype(F32)
    new_weights = weights * (1.0 - LEARN_RATE * WEIGHT_DECAY) - LEARN_RATE * update
    return (new_weights, new_momentum, update)


def solution(mesh):
    fine = Mesh(mesh.devices.reshape(4, 2, 2, 4, 2), ("z", "xh", "xp", "y", "c"))
    spec = P(None, ("z", "xh", "xp"), ("y", "c"))
    return jax.shard_map(
        per_device, mesh=fine, in_specs=(spec, spec, spec), out_specs=(spec, spec, spec), check_vma=False
    )
```

time: 568 us -> 297 us (0.52)
  waiting for transfers between devices: 294 us -> 18.8 us
  blocking collectives: 214 us -> 168 us
  matrix products: 39.3 us -> 68.3 us
  other arithmetic: 5.28 us -> 19.5 us
  between operations: 14.2 us -> 1.72 us
  local copies, waits for them, and re-layouts: 0.01 us -> 10.7 us
  starting transfers between devices: 0.29 us -> 9.49 us
    psum x3 -> x0, blocking collectives: 214 us -> none  [the longest x2 201 us: per_device(): gram_rows = lax.psum(partial_value, 'fs')]
    all_gather x6 -> x0, waiting for transfers between devices: 190 us -> none  [the longest x3 96.3 us: per_device(): row_whole = lax.all_gather(plain, 'tp', axis=2, tiled=True)]
    all_to_all x0 -> x5, blocking collectives: none -> 168 us  [the longest x3 133 us: gather(): lax.all_to_all(spread, axes, split_axis=0, concat_axis=0, tiled=False)]
    psum x1 -> x0, waiting for transfers between devices: 104 us -> none  [per_device(): gram_rows = lax.psum(partial_value, 'fs')]
    dot_general x9 -> x15, matrix products: 39.3 us -> 68.3 us  [the longest x14 67.3 us: dot(): return jnp.dot(left, right, preferred_element_type=F32)]
    ppermute x0 -> x5, waiting for transfers between devices: none -> 18.8 us  [swap(): return lax.ppermute(value, axis, [(0, 1), (1, 0)])]
    ppermute x0 -> x5, starting transfers between devices: none -> 9.49 us  [swap(): return lax.ppermute(value, axis, [(0, 1), (1, 0)])]
    select_n x0 -> x5, other arithmetic: none -> 8.64 us  [the longest x2 6.59 us: whole_gram(): first = jnp.where(core == 0, part, other)]
  transfers between devices with their start and end apart: 7 -> 5, of which waited for: 7 -> 4; matrix products, arithmetic and copies ran while one was open for 0% -> 2% of each run, Pallas kernels for 0% -> 0%
where the time goes in v1:
time: 297 us; the launch traced here: 296 us
  blocking collectives  168 us (57%)
  matrix products  68.3 us (23%)
  other arithmetic  19.5 us (7%)
  waiting for transfers between devices  18.8 us (6%)
  local copies, waits for them, and re-layouts  10.7 us (4%)
  starting transfers between devices  9.49 us (3%)
    all_to_all x3, blocking collectives, gather(): lax.all_to_all(spread, axes, split_axis=0, concat_axis=0, tiled=False)  133 us
    dot_general x14, matrix products, dot(): return jnp.dot(left, right, preferred_element_type=F32)  67.3 us
    all_to_all x1, blocking collectives, per_device(): pieces = lax.all_to_all(partial, ('z', 'xh'), split_axis=0, concat_axis=0)  23.9 us
    ppermute x5, waiting for transfers between devices, swap(): return lax.ppermute(value, axis, [(0, 1), (1, 0)])  18.8 us
    all_to_all x1, blocking collectives, per_device(): lax.all_to_all(back, ('c', 'y'), split_axis=0, concat_axis=0)  10.1 us
    ppermute x5, starting transfers between devices, swap(): return lax.ppermute(value, axis, [(0, 1), (1, 0)])  9.49 us
    select_n x2, other arithmetic, whole_gram(): first = jnp.where(core == 0, part, other)  6.59 us
  transfers between devices with their start and end apart: 5, of which 4 were waited for; matrix products, arithmetic and copies ran while one was open for 2% of the time, Pallas kernels for 0%

profile of v1, /device:TPU:1, one launch (start us, length us, event | category | flops | bytes accessed | tf_op | source)
XLA Modules:
  0.0 296.1 jit_solution(10606282718862768060)
XLA Ops:
  0.6 2.3 add_convert_fusion.2
  5.1 3.8 %collective-permute-done = bf16[352,256]{1,0:T(8,128)(2,1)S(1)} collective-permute-done((bf16[352,256]{1,0:T(8,128)(2,1)S(1)}, bf16[352,256]{1,0:T(8,128)(2,1)S(1)}, u32[]{:S(2)}, u32[]{:S(2)}) %collective-permute-start) | collective-permute-done | bytes 180256 | tf_op jit(solution)/shard_map/ppermute | solution.py:31
  9.1 22.0 %all_to_all.25 = bf16[4,704,256]{2,1,0:T(8,128)(2,1)S(1)} all-to-all(bf16[4,704,256]{2,1,0:T(8,128)(2,1)S(1)} %broadcast_in_dim.6), channel_id=1, replica_groups=mesh['z'=4,'xh'=2,'xp'=2,'y'=4,'c'=2] {'y'}, dimensions={0} | all-to-all | bytes 2883584 | tf_op jit(solution)/shard_map/all_to_all | solution.py:27
  31.0 2.7 collective-permute-start.1
  33.7 3.0 %collective-permute-done.1 = bf16[4,704,256]{2,1,0:T(8,128)(2,1)} collective-permute-done((bf16[4,704,256]{2,1,0:T(8,128)(2,1)S(1)}, bf16[4,704,256]{2,1,0:T(8,128)(2,1)}, u32[]{:S(2)}, u32[]{:S(2)}) %collective-permute-start.1) | collective-permute-done | bytes 1441824 | tf_op jit(solution)/shard_map/ppermute | solution.py:31
  41.2 2.3 reshape.31
  43.6 23.9 %all_to_all.26 = bf16[8,32,2048]{2,1,0:T(8,128)(2,1)} all-to-all(bf16[8,32,2048]{2,1,0:T(8,128)(2,1)} %reshape.31), channel_id=1, replica_groups=mesh['z'=4,'xh'=2,'xp'=2,'y'=4,'c'=2] {'z','xh'}, dimensions={0} | all-to-all | bytes 2097152 | tf_op jit(solution)/shard_map/all_to_all | solution.py:79
  69.4 55.3 %all_to_all.27 = bf16[32,32,2048]{2,1,0:T(8,128)(2,1)S(1)} all-to-all(bf16[32,32,2048]{2,1,0:T(8,128)(2,1)S(1)} %broadcast_in_dim.7), channel_id=1, replica_groups=mesh['z'=4,'xh'=2,'xp'=2,'y'=4,'c'=2] {'y','z','xh'}, dimensions={0} | all-to-all | bytes 8388608 | tf_op jit(solution)/shard_map/all_to_all | solution.py:27
  124.7 2.6 collective-permute-start.2
  127.3 6.8 %collective-permute-done.2 = bf16[1024,2048]{1,0:T(8,128)(2,1)S(1)} collective-permute-done((bf16[1024,2048]{1,0:T(8,128)(2,1)S(1)}, bf16[1024,2048]{1,0:T(8,128)(2,1)S(1)}, u32[]{:S(2)}, u32[]{:S(2)}) %collective-permute-start.2) | collective-permute-done | bytes 4194336 | tf_op jit(solution)/shard_map/ppermute | solution.py:31
  138.2 4.9 %multiply_reduce_fusion = f32[]{:T(128)} fusion(bf16[1024,2048]{1,0:T(8,128)(2,1)S(1)} %get-tuple-element.20, bf16[1024,2048]{1,0:T(8,128)(2,1)S(1)} %get-tuple-element.19), kind=kLoop, calls=%fused_computation | loop fusion | flops 25165824 | bytes 8388612 | tf_op jit(solution)/shard_map/reduce_sum | solution.py:83
  143.9 4.3 %convolution_multiply_fusion.8 = f32[32,2048]{1,0:T(8,128)S(1)} fusion(bf16[32,2048]{1,0:T(8,128)(2,1)S(1)} %reduce_sum.21, f32[]{:T(128)S(6)} %mul.165, bf16[1024,2048]{1,0:T(8,128)(2,1)} %copy-done.2, bf16[1024,2048]{1,0:T(8,128)(2,1)} %copy-done), kind=kOutput, calls=%fused_computation.25 | convolution fusion | flops 285278208 | bytes 8781828 | tf_op jit(solution)/shard_map/dot_general | solution.py:35
  148.2 4.3 %fusion.6 = f32[32,2048]{1,0:T(8,128)S(1)} fusion(f32[32,2048]{1,0:T(8,128)S(1)} %convolution_multiply_fusion.8, bf16[32,2048]{1,0:T(8,128)(2,1)S(1)} %reduce_sum.21, f32[]{:T(128)S(6)} %mul.169, f32[]{:T(128)S(6)} %mul.165, bf16[1024,2048]{1,0:T(8,128)(2,1)} %copy-done.2, bf16[1024,2048]{1,0:T(8,128)(2,1)} %copy-done), kind=kOutput, calls=%fused_computation.26 | convolution fusion | flops 285736960 | bytes 9043976 | tf_op jit(solution)/shard_map/dot_general | solution.py:35
  152.6 9.0 %fusion.7 = bf16[32,2048]{1,0:T(8,128)(2,1)S(1)} fusion(f32[32,2048]{1,0:T(8,128)S(1)} %fusion.6, f32[]{:T(128)S(6)} %mul.165, bf16[1024,2048]{1,0:T(8,128)(2,1)} %copy-done.2, bf16[1024,2048]{1,0:T(8,128)(2,1)} %copy-done), kind=kOutput, calls=%fused_computation.27 | convolution fusion | flops 571080704 | bytes 8781828 | tf_op jit(solution)/shard_map/dot_general | solution.py:35
  162.1 56.2 %all_to_all.28 = bf16[32,32,2048]{2,1,0:T(8,128)(2,1)} all-to-all(bf16[32,32,2048]{2,1,0:T(8,128)(2,1)S(1)} %broadcast_in_dim.8), channel_id=1, replica_groups=mesh['z'=4,'xh'=2,'xp'=2,'y'=4,'c'=2] {'y','z','xh'}, dimensions={0} | all-to-all | bytes 8388608 | tf_op jit(solution)/shard_map/all_to_all | solution.py:27
  219.9 4.4 %convolution_multiply_fusion.4 = f32[88,2048]{1,0:T(8,128)S(1)} fusion(bf16[88,2048]{1,0:T(8,128)(2,1)S(1)} %bitcast.37, f32[]{:T(128)S(6)} %mul.165, bf16[1024,2048]{1,0:T(8,128)(2,1)} %copy-done.2, bf16[1024,2048]{1,0:T(8,128)(2,1)} %copy-done), kind=kOutput, calls=%fused_computation.15 | convolution fusion | flops 755154944 | bytes 9469956 | tf_op jit(solution)/shard_map/dot_general | solution.py:35
  227.4 5.7 %broadcast_select_fusion.1 = (bf16[1024,2048]{1,0:T(8,128)(2,1)}, bf16[1024,2048]{1,0:T(8,128)(2,1)}) fusion(bf16[1024,2048]{1,0:T(8,128)(2,1)} %collective-permute-done.3, pred[]{:T(512)S(6)} %eq.5, bf16[32,32,2048]{2,1,0:T(8,128)(2,1)} %all_to_all.28), kind=kLoop, calls=%fused_computation.4 | loop fusion | flops 4194304 | bytes 16777216 | tf_op jit(solution)/shard_map/jit(_where)/select_n | solution.py:53
  233.1 9.3 %convolution_add_fusion = f32[88,2048]{1,0:T(8,128)S(1)} fusion(f32[88,2048]{1,0:T(8,128)S(1)} %convolution_multiply_fusion.3, f32[88,2048]{1,0:T(8,128)S(1)} %convolution_multiply_fusion.4, bf16[88,2048]{1,0:T(8,128)(2,1)S(1)} %bitcast.38, f32[]{:T(128)S(6)} %div.7, bf16[1024,2048]{1,0:T(8,128)(2,1)} %get-tuple-element.18, ...), kind=kOutput, calls=%fused_computation.17 | convolution fusion | flops 1514455040 | bytes 10911748 | tf_op jit(solution)/shard_map/dot_general | solution.py:35
  242.4 4.3 %fusion.46 = f32[88,2048]{1,0:T(8,128)S(1)} fusion(f32[88,2048]{1,0:T(8,128)S(1)} %convolution_add_fusion, bf16[1024,2048]{1,0:T(8,128)(2,1)} %get-tuple-element.18, bf16[1024,2048]{1,0:T(8,128)(2,1)} %get-tuple-element.17), kind=kOutput, calls=%fused_computation.88 | convolution fusion | flops 755154944 | bytes 9830400 | tf_op jit(solution)/shard_map/dot_general | solution.py:35
  246.7 9.1 %multiply_add_fusion.1 = f32[88,2048]{1,0:T(8,128)S(1)} fusion(f32[88,2048]{1,0:T(8,128)S(1)} %fusion.46, bf16[1024,2048]{1,0:T(8,128)(2,1)} %get-tuple-element.18, bf16[1024,2048]{1,0:T(8,128)(2,1)} %get-tuple-element.17), kind=kOutput, calls=%fused_computation.75 | convolution fusion | flops 1511211008 | bytes 9830400 | tf_op jit(solution)/shard_map/dot_general | solution.py:35
  255.9 9.2 %subtract_convert_fusion.4 = (bf16[88,2048]{1,0:T(8,128)(2,1)S(1)}, bf16[88,2048]{1,0:T(8,128)(2,1)S(1)}) fusion(bf16[1024,2048]{1,0:T(8,128)(2,1)} %get-tuple-element.18, bf16[1024,2048]{1,0:T(8,128)(2,1)} %get-tuple-element.17, f32[88,2048]{1,0:T(8,128)S(1)} %multiply_add_fusion.1, f32[88,2048]{1,0:T(8,128)S(1)} %convolution_add_fusion), kind=kOutput, calls=%fused_computation.71 | convolution fusion | flops 1512472576 | bytes 10551296 | tf_op jit(solution)/shard_map/dot_general | solution.py:35
  265.1 4.8 %fusion.18 = f32[176,2048]{1,0:T(8,128)S(1)} fusion(bf16[88,2048]{1,0:T(8,128)(2,1)S(1)} %get-tuple-element.13, bf16[88,2048]{1,0:T(8,128)(2,1)S(1)} %get-tuple-element.14, bf16[1024,2048]{1,0:T(8,128)(2,1)} %get-tuple-element.18, bf16[1024,2048]{1,0:T(8,128)(2,1)} %get-tuple-element.17), kind=kOutput, calls=%fused_computation.47 | convolution fusion | flops 1494614016 | bytes 10551296 | tf_op jit(solution)/shard_map/dot_general | solution.py:35
  278.8 10.1 %all_to_all.29 = bf16[8,88,256]{2,1,0:T(8,128)(2,1)S(1)} all-to-all(bf16[8,88,256]{2,1,0:T(8,128)(2,1)S(1)} %bitcast.34), channel_id=1, replica_groups=mesh['z'=4,'xh'=2,'xp'=2,'y'=4,'c'=2] {'c','y'}, dimensions={0} | all-to-all | bytes 720896 | tf_op jit(solution)/shard_map/all_to_all | solution.py:109
  289.6 5.2 %collective-permute-done.4 = bf16[352,256]{1,0:T(8,128)(2,1)S(1)} collective-permute-done((bf16[352,256]{1,0:T(8,128)(2,1)S(1)}, bf16[352,256]{1,0:T(8,128)(2,1)S(1)}, u32[]{:S(2)}, u32[]{:S(2)}) %collective-permute-start.4) | collective-permute-done | bytes 180256 | tf_op jit(solution)/shard_map/ppermute | solution.py:31
  (46 shorter events, 28.6 us)
Async XLA Ops:
  3.0 5.9 %collective-permute-start = (bf16[352,256]{1,0:T(8,128)(2,1)S(1)}, bf16[352,256]{1,0:T(8,128)(2,1)S(1)}, u32[]{:S(2)}, u32[]{:S(2)}) collective-permute-start(bf16[352,256]{1,0:T(8,128)(2,1)S(1)} %get-tuple-element.30), channel_id=1, source_target_pairs={{0,8},{8,0},{1,9},{9,1},{2,10},{10,2},{3,11},{11,3},{4,12},{12,4},... | collective-permute-start | bytes 540680 | tf_op jit(solution)/shard_map/ppermute | solution.py:31
  31.0 2.7 copy-start.4
  31.0 5.6 %collective-permute-start.1 = (bf16[4,704,256]{2,1,0:T(8,128)(2,1)S(1)}, bf16[4,704,256]{2,1,0:T(8,128)(2,1)}, u32[]{:S(2)}, u32[]{:S(2)}) collective-permute-start(bf16[4,704,256]{2,1,0:T(8,128)(2,1)S(1)} %all_to_all.25), channel_id=1, source_target_pairs={{0,1},{1,0},{2,3},{3,2},{4,5},{5,4},{6,7},{7,6},{8,9},{9,8},{10,11... | collective-permute-start | bytes 4325384 | tf_op jit(solution)/shard_map/ppermute | solution.py:31
  124.7 9.4 %collective-permute-start.2 = (bf16[1024,2048]{1,0:T(8,128)(2,1)S(1)}, bf16[1024,2048]{1,0:T(8,128)(2,1)S(1)}, u32[]{:S(2)}, u32[]{:S(2)}) collective-permute-start(bf16[1024,2048]{1,0:T(8,128)(2,1)S(1)} %bitcast.32), channel_id=1, source_target_pairs={{0,1},{1,0},{2,3},{3,2},{4,5},{5,4},{6,7},{7,6},{8,9},{9,8},{10,11... | collective-permute-start | bytes 12582920 | tf_op jit(solution)/shard_map/ppermute | solution.py:31
  135.0 1.9 copy-start
  135.0 3.2 %copy-start.2 = (bf16[1024,2048]{1,0:T(8,128)(2,1)}, bf16[1024,2048]{1,0:T(8,128)(2,1)S(1)}, u32[]{:S(2)}) copy-start(bf16[1024,2048]{1,0:T(8,128)(2,1)S(1)} %get-tuple-element.20) | copy-start | bytes 12582916
  218.3 9.1 %collective-permute-start.3 = (bf16[1024,2048]{1,0:T(8,128)(2,1)}, bf16[1024,2048]{1,0:T(8,128)(2,1)}, u32[]{:S(2)}, u32[]{:S(2)}) collective-permute-start(bf16[1024,2048]{1,0:T(8,128)(2,1)} %bitcast.5), channel_id=1, source_target_pairs={{0,1},{1,0},{2,3},{3,2},{4,5},{5,4},{6,7},{7,6},{8,9},{9,8},{10,11... | collective-permute-start | bytes 12582920 | tf_op jit(solution)/shard_map/ppermute | solution.py:31
  219.9 4.7 %copy-start.1 = (bf16[1024,2048]{1,0:T(8,128)(2,1)S(1)}, bf16[1024,2048]{1,0:T(8,128)(2,1)}, u32[]{:S(2)}) copy-start(bf16[1024,2048]{1,0:T(8,128)(2,1)} %copy-done) | copy-start | bytes 12582916
  219.9 5.9 %copy-start.3 = (bf16[1024,2048]{1,0:T(8,128)(2,1)S(1)}, bf16[1024,2048]{1,0:T(8,128)(2,1)}, u32[]{:S(2)}) copy-start(bf16[1024,2048]{1,0:T(8,128)(2,1)} %copy-done.2) | copy-start | bytes 12582916
  265.1 5.0 %copy-start.5 = (bf16[1024,2048]{1,0:T(8,128)(2,1)S(1)}, bf16[1024,2048]{1,0:T(8,128)(2,1)}, u32[]{:S(2)}) copy-start(bf16[1024,2048]{1,0:T(8,128)(2,1)} %get-tuple-element.17) | copy-start | bytes 12582916
  265.1 5.9 %copy-start.6 = (bf16[1024,2048]{1,0:T(8,128)(2,1)S(1)}, bf16[1024,2048]{1,0:T(8,128)(2,1)}, u32[]{:S(2)}) copy-start(bf16[1024,2048]{1,0:T(8,128)(2,1)} %get-tuple-element.18) | copy-start | bytes 12582916
  278.5 16.3 %copy-start.7 = (f32[2,352,256]{2,1,0:T(8,128)S(1)}, f32[2,352,256]{2,1,0:T(8,128)}, u32[]{:S(2)}) copy-start(f32[2,352,256]{2,1,0:T(8,128)} %param.3) | copy-start | bytes 2162692
  289.0 5.8 %collective-permute-start.4 = (bf16[352,256]{1,0:T(8,128)(2,1)S(1)}, bf16[352,256]{1,0:T(8,128)(2,1)S(1)}, u32[]{:S(2)}, u32[]{:S(2)}) collective-permute-start(bf16[352,256]{1,0:T(8,128)(2,1)S(1)} %bitcast.39), channel_id=1, source_target_pairs={{0,8},{8,0},{1,9},{9,1},{2,10},{10,2},{3,11},{11,3},{4,12},{12,4},... | collective-permute-start | bytes 540680 | tf_op jit(solution)/shard_map/ppermute | solution.py:31

commit v2 on v1

v2 whole, which is shorter than its diff:
```python
import math

import jax
import jax.numpy as jnp
from jax import lax
from jax.experimental import pallas as pl
from jax.experimental.pallas import tpu as pltpu
from jax.sharding import Mesh, PartitionSpec as P

D = 2048
FF = 5632

MOMENTUM_DECAY = 0.95
A1 = 3.4445
A2 = -4.775
A3 = 2.0315
LEARN_RATE = 0.02
WEIGHT_DECAY = 0.1
EPSILON = 1e-07
STEP_SCALE = 0.2
NORM_SAFETY = 1.8

BF = jnp.bfloat16
F32 = jnp.float32

ROWS = 88
GROWS = 32
BLK = 256
PACK = 5 * BLK
TILE = 512
LOW = 96

VMEM = pl.BlockSpec(memory_space=pltpu.VMEM)
SMEM = pl.BlockSpec(memory_space=pltpu.SMEM)


def at(start, size):
    return pl.ds(pl.multiple_of(start, size), size)


def gather(value, axes, count):
    spread = jnp.broadcast_to(value[None], (count,) + value.shape)
    return lax.all_to_all(spread, axes, split_axis=0, concat_axis=0, tiled=False)


def swap(value, axis):
    return lax.ppermute(value, axis, [(0, 1), (1, 0)])


def unpack(full, own, other, core):
    for part, base in ((own, core * 4), (other, (1 - core) * 4)):

        def panel(k, carry, part=part, base=base):
            here = base + k
            for d in range(5):
                there = lax.rem(here + d, 8)
                block = part[at(k * BLK, BLK), d * BLK : (d + 1) * BLK]
                full[at(here * BLK, BLK), at(there * BLK, BLK)] = block
                if 0 < d < 4:
                    full[at(there * BLK, BLK), at(here * BLK, BLK)] = block.T
            return carry

        lax.fori_loop(0, 4, panel, 0)


def square_sum(parts):
    total = jnp.zeros((1, BLK), F32)
    for part in parts:

        def panel(k, total, part=part):
            for d in range(5):
                block = part[at(k * BLK, BLK), d * BLK : (d + 1) * BLK].astype(F32)
                value = jnp.sum(block * block, axis=0, keepdims=True)
                total = total + (2.0 * value if 0 < d < 4 else value)
            return total

        total = lax.fori_loop(0, 4, panel, total)
    return jnp.sum(total, axis=1, keepdims=True)


def columns(body):
    def step(n, carry):
        body(at(n * TILE, TILE))
        return carry

    lax.fori_loop(0, D // TILE, step, 0)


def dot(left, right):
    return jnp.dot(left, right, preferred_element_type=F32)


def gram_kernel(where, b0, b1, b2, b3, out, rows_out, whole):
    core, half = where[0], where[1]
    slot = core * 2 + half
    away = (1 - core) * 2
    whole[:, at(slot * TILE, TILE)] = b0[...]
    whole[:, at((core * 2 + 1 - half) * TILE, TILE)] = b1[...]
    whole[:, at((away + half) * TILE, TILE)] = b2[...]
    whole[:, at((away + 1 - half) * TILE, TILE)] = b3[...]
    for i in range(2):
        left = b0[:, i * BLK : (i + 1) * BLK].T
        here = slot * 2 + i

        def block(d, carry, i=i, left=left, here=here):
            there = lax.rem(here + d, 8)
            value = dot(left, whole[:, at(there * BLK, BLK)])
            out[i * BLK : (i + 1) * BLK, at(d * BLK, BLK)] = value.astype(BF)
            return carry

        lax.fori_loop(0, 5, block, 0)
    for k in range(4):

        @pl.when(slot == k)
        def _(k=k):
            rows_out[...] = whole[k * ROWS : (k + 1) * ROWS, :]


def first_kernel(where, own, other, plain, rows_out, x_out, full, l1, l2, u, hold, w, g1):
    core, row = where[0], where[1]
    unpack(full, own, other, core)
    squares = square_sum((own, other))
    ratio = 1.0 / (NORM_SAFETY * jnp.sqrt(jnp.sqrt(squares / D)) + EPSILON)
    q = ratio * ratio
    l1[:GROWS, :] = full[at(row, GROWS), :]
    l1[GROWS:, :] = plain[...]

    def one(sl):
        value = q * dot(l1[...], full[:, sl])
        u[:, sl] = value
        l2[:, sl] = value.astype(BF)

    columns(one)

    def two(sl):
        value = q * dot(l2[...], full[:, sl])
        mixed = A1 * l1[:, sl].astype(F32) + A2 * u[:, sl] + A3 * value
        x_out[:, sl] = ratio * mixed[GROWS:]
        kept = q * mixed[:GROWS]
        hold[:, sl] = kept
        l1[:GROWS, sl] = kept.astype(BF)

    columns(two)

    def three(sl):
        value = q * dot(l1[:GROWS, :], full[:, sl])
        w[:, sl] = value
        l2[:GROWS, sl] = value.astype(BF)

    columns(three)

    def four(sl):
        value = q * dot(l2[:GROWS, :], full[:, sl])
        g1[:, sl] = (A1 * hold[:, sl] + A2 * w[:, sl] + A3 * value).astype(BF)

    columns(four)
    here = row // BLK
    for d in range(5):
        rows_out[:, d * BLK : (d + 1) * BLK] = g1[:, at(lax.rem(here + d, 8) * BLK, BLK)]


def second_kernel(where, own, other, x1, out, full, la, lb, v, w, x2, y):
    core = where[0]
    unpack(full, own, other, core)
    lefts = (la, lb)

    def put(left, sl, value, split):
        high = value.astype(BF)
        left[:ROWS, sl] = high
        if split:
            left[LOW : LOW + ROWS, sl] = (value - high.astype(F32)).astype(BF)

    turn = [0]

    def times(finish, split, next_split):
        src, dst = lefts[turn[0]], lefts[1 - turn[0]]
        turn[0] = 1 - turn[0]

        def body(sl):
            if split:
                both = dot(src[...], full[:, sl])
                value = both[:ROWS] + both[LOW : LOW + ROWS]
            else:
                value = dot(src[:ROWS, :], full[:, sl])
            value = finish(sl, value)
            if next_split is not None:
                put(dst, sl, value, next_split)

        columns(body)

    def keep(ref):
        def finish(sl, value):
            ref[:, sl] = value
            return value

        return finish

    def mix(start, ref):
        def finish(sl, value):
            value = A1 * start[:, sl] + A2 * w[:, sl] + A3 * value
            if ref is not None:
                ref[:, sl] = value
            return value

        return finish

    la[ROWS:, :] = jnp.zeros((la.shape[0] - ROWS, D), BF)
    lb[ROWS:, :] = jnp.zeros((lb.shape[0] - ROWS, D), BF)
    la[:ROWS, :] = x1[...].astype(BF)

    times(keep(w), False, False)
    times(mix(x1, x2), False, False)
    s = False
    times(keep(v), s, s)
    times(keep(w), s, s)
    times(mix(v, v), s, s)
    times(keep(w), s, s)
    times(mix(v, y), s, True)
    s = True
    times(keep(v), s, s)
    times(keep(w), s, s)
    times(mix(v, v), s, s)
    times(keep(w), s, s)

    def last(sl, value):
        value = A1 * v[:, sl] + A2 * w[:, sl] + A3 * value
        out[:, sl] = (A1 * x2[:, sl] + A2 * y[:, sl] + A3 * value).astype(BF)
        return None

    times(last, s, None)


def call(kernel, outs, scratch, where, *args):
    return pl.pallas_call(
        kernel,
        out_shape=outs,
        in_specs=[SMEM] + [VMEM] * len(args),
        out_specs=[VMEM] * len(outs),
        scratch_shapes=scratch,
        compiler_params=pltpu.CompilerParams(vmem_limit_bytes=60 * 1024 * 1024),
    )(where, *args)


def shape(dims, dtype):
    return jax.ShapeDtypeStruct(dims, dtype)


def per_device(weights, momentum, gradients):
    mat = lax.axis_index("m")
    core = lax.axis_index("c")
    half = lax.axis_index("y0")
    row = core * 1024 + half * 512 + (lax.axis_index("z") * 4 + lax.axis_index("x")) * GROWS
    where = jnp.stack([core, half]).astype(jnp.int32)
    where_row = jnp.stack([core, row]).astype(jnp.int32)

    new_momentum = MOMENTUM_DECAY * momentum + gradients
    iterate = gradients + MOMENTUM_DECAY * new_momentum
    plain = iterate.astype(BF)

    mine = jnp.where(mat == 0, plain[0], plain[1])
    other = jnp.where(mat == 0, plain[1], plain[0])
    block = jnp.concatenate([mine, swap(other, "m")], 1)
    near = swap(block, "y0")
    far = swap(block, "c")
    diagonal = swap(near, "c")

    partial, own_rows = call(
        gram_kernel,
        (shape((2 * BLK, PACK), BF), shape((ROWS, D), BF)),
        [pltpu.VMEM((352, D), BF)],
        where, block, near, far, diagonal,
    )
    pieces = lax.all_to_all(partial.reshape(16, GROWS, PACK), ("z", "x"), split_axis=0, concat_axis=0)
    gram_rows = jnp.sum(pieces.astype(F32), axis=0).astype(BF)

    def whole(rows):
        part = gather(rows, ("y0", "z", "x"), 32).reshape(1024, PACK)
        return part, swap(part, "c")

    own, away = whole(gram_rows)
    next_rows, x1 = call(
        first_kernel,
        (shape((GROWS, PACK), BF), shape((ROWS, D), F32)),
        [
            pltpu.VMEM((D, D), BF),
            pltpu.VMEM((GROWS + ROWS, D), BF),
            pltpu.VMEM((GROWS + ROWS, D), BF),
            pltpu.VMEM((GROWS + ROWS, D), F32),
            pltpu.VMEM((GROWS, D), F32),
            pltpu.VMEM((GROWS, D), F32),
            pltpu.VMEM((GROWS, D), BF),
        ],
        where_row, own, away, own_rows,
    )
    own, away = whole(next_rows)
    (x3,) = call(
        second_kernel,
        (shape((ROWS, D), BF),),
        [pltpu.VMEM((D, D), BF)]
        + [pltpu.VMEM((2 * LOW, D), BF)] * 2
        + [pltpu.VMEM((ROWS, D), F32)] * 4,
        where_row, own, away, x1,
    )

    back = x3.reshape(ROWS, 4, TILE).transpose(1, 0, 2)
    back = lax.all_to_all(back, ("c", "y0"), split_axis=0, concat_axis=0).reshape(352, TILE)
    kept = back[:, :BLK]
    came = swap(back[:, BLK:], "m")
    both = jnp.stack([jnp.where(mat == 0, kept, came), jnp.where(mat == 0, came, kept)])

    update = STEP_SCALE * math.sqrt(max(FF, D)) * both.astype(F32)
    new_weights = weights * (1.0 - LEARN_RATE * WEIGHT_DECAY) - LEARN_RATE * update
    return (new_weights, new_momentum, update)


def solution(mesh):
    fine = Mesh(mesh.devices.reshape(4, 4, 2, 2, 2), ("z", "x", "m", "y0", "c"))
    spec = P(None, ("z", "x"), ("m", "y0", "c"))
    return jax.shard_map(
        per_device, mesh=fine, in_specs=(spec, spec, spec), out_specs=(spec, spec, spec), check_vma=False
    )
```

time: 297 us -> 209 us (0.70)
  matrix products: 68.3 us -> 0 us
  blocking collectives: 168 us -> 109 us
  Pallas kernels: 0 us -> 48.9 us
  other arithmetic: 19.5 us -> 5.05 us
  starting transfers between devices: 9.49 us -> 16.7 us
  local copies, waits for them, and re-layouts: 10.7 us -> 4.88 us
  waiting for transfers between devices: 18.8 us -> 22.8 us
    dot_general x15 -> x0, matrix products: 68.3 us -> none  [the longest x14 67.3 us: dot(): return jnp.dot(left, right, preferred_element_type=F32)]
    all_to_all x3 -> x2, blocking collectives: 133 us -> 73.1 us  [gather(): lax.all_to_all(spread, axes, split_axis=0, concat_axis=0, tiled=False)]
    pallas_call x0 -> x3, Pallas kernels: none -> 48.9 us  [call(): pl.pallas_call(kernel, out_shape=outs, in_specs=[SMEM] + [VMEM] * len(arg...]
    select_n x4 -> x0, other arithmetic: 8.61 us -> none  [the longest x2 6.59 us: whole_gram(): first = jnp.where(core == 0, part, other)]
    ppermute x5 -> x7, starting transfers between devices: 9.49 us -> 16.7 us  [swap(): return lax.ppermute(value, axis, [(0, 1), (1, 0)])]
    reduce_sum x1 -> x0, other arithmetic: 4.93 us -> none  [per_device(): squares = jnp.sum(jnp.square(gram.astype(F32)))]
    ppermute x5 -> x7, waiting for transfers between devices: 18.8 us -> 22.8 us  [swap(): return lax.ppermute(value, axis, [(0, 1), (1, 0)])]
    unnamed x16, local copies, waits for them, and re-layouts: 5.65 us -> 2.33 us
  transfers between devices with their start and end apart: 5 -> 7, of which waited for: 4 -> 6; matrix products, arithmetic and copies ran while one was open for 2% -> 1% of each run, Pallas kernels for 0% -> 0%
where the time goes in v2:
time: 209 us; the launch traced here: 208 us
  blocking collectives  109 us (52%)
  Pallas kernels  48.9 us (23%)
  waiting for transfers between devices  22.8 us (11%)
  starting transfers between devices  16.7 us (8%)
  other arithmetic  5.05 us (2%)
  local copies, waits for them, and re-layouts  4.88 us (2%)
    all_to_all x2, blocking collectives, gather(): lax.all_to_all(spread, axes, split_axis=0, concat_axis=0, tiled=False)  73.1 us
    pallas_call x3, Pallas kernels, call(): pl.pallas_call(kernel, out_shape=outs, in_specs=[SMEM] + [VMEM] * len(arg...  48.9 us
    all_to_all x1, blocking collectives, per_device(): lax.all_to_all(partial.reshape(16, GROWS, PACK), ('z', 'x'), split_axis=0...  27.1 us
    ppermute x7, waiting for transfers between devices, swap(): return lax.ppermute(value, axis, [(0, 1), (1, 0)])  22.8 us
    ppermute x7, starting transfers between devices, swap(): return lax.ppermute(value, axis, [(0, 1), (1, 0)])  16.7 us
    all_to_all x1, blocking collectives, per_device(): lax.all_to_all(back, ('c', 'y0'), split_axis=0, concat_axis=0)  8.89 us
  transfers between devices with their start and end apart: 7, of which 6 were waited for; matrix products, arithmetic and copies ran while one was open for 1% of the time, Pallas kernels for 0%

profile of v2, /device:TPU:1, one launch (start us, length us, event | category | flops | bytes accessed | tf_op | source)
XLA Modules:
  0.0 208.2 jit_solution(18243754391773748600)
XLA Ops:
  0.6 2.3 %add_convert_fusion = (bf16[2,352,256]{2,1,0:T(8,128)(2,1)S(1)}, f32[2,352,256]{2,1,0:T(8,128)}) fusion(f32[2,352,256]{2,1,0:T(8,128)} %param.5, f32[2,352,256]{2,1,0:T(8,128)} %param.4), kind=kLoop, calls=%fused_computation.3 | loop fusion | flops 901120 | bytes 2523136 | tf_op jit(solution)/shard_map/convert_element_type | solution.py:258
  3.0 3.8 %collective-permute-start = (bf16[352,256]{1,0:T(8,128)(2,1)S(1)}, bf16[352,256]{1,0:T(8,128)(2,1)S(1)}, u32[]{:S(2)}, u32[]{:S(2)}) collective-permute-start(bf16[352,256]{1,0:T(8,128)(2,1)S(1)} %get-tuple-element.18), channel_id=1, source_target_pairs={{0,4},{4,0},{1,5},{5,1},{2,6},{6,2},{3,7},{7,3},{8,12},{12,8},{9,1... | collective-permute-start | bytes 540680 | tf_op jit(solution)/shard_map/ppermute | solution.py:47
  6.8 4.0 %collective-permute-done = bf16[352,256]{1,0:T(8,128)(2,1)S(1)} collective-permute-done((bf16[352,256]{1,0:T(8,128)(2,1)S(1)}, bf16[352,256]{1,0:T(8,128)(2,1)S(1)}, u32[]{:S(2)}, u32[]{:S(2)}) %collective-permute-start) | collective-permute-done | bytes 180256 | tf_op jit(solution)/shard_map/ppermute | solution.py:47
  10.9 1.4 collective-permute-start.1
  12.2 1.8 collective-permute-start.2
  14.1 5.4 %collective-permute-done.1.b1 = bf16[352,512]{1,0:T(8,128)(2,1)S(1)} collective-permute-done((bf16[352,512]{1,0:T(8,128)(2,1)S(1)}, bf16[352,512]{1,0:T(8,128)(2,1)S(1)}, u32[]{:S(2)}, u32[]{:S(2)}) %collective-permute-start.1) | collective-permute-done | bytes 360480 | tf_op jit(solution)/shard_map/ppermute | solution.py:47
  19.5 2.3 %collective-permute-start.3 = (bf16[352,512]{1,0:T(8,128)(2,1)S(1)}, bf16[352,512]{1,0:T(8,128)(2,1)S(1)}, u32[]{:S(2)}, u32[]{:S(2)}) collective-permute-start(bf16[352,512]{1,0:T(8,128)(2,1)S(1)} %collective-permute-done.1.b1), channel_id=1, source_target_pairs={{0,1},{1,0},{2,3},{3,2},{4,5},{5,4},{6,7},{7,6},{8,9},{9,8},{10,11... | collective-permute-start | bytes 1081352 | tf_op jit(solution)/shard_map/ppermute | solution.py:47
  23.9 5.1 %shard_map.58 = (bf16[512,1280]{1,0:T(8,128)(2,1)}, bf16[88,2048]{1,0:T(8,128)(2,1)}) custom-call(s32[2]{0:T(128)} %pad_add_fusion.1.where, bf16[352,512]{1,0:T(8,128)(2,1)} %copy-done.3, bf16[352,512]{1,0:T(8,128)(2,1)} %copy-done.5, bf16[352,512]{1,0:T(8,128)(2,1)} %copy-done.6, bf16[352,512]{1,0:T(8,128)(2,1)} %copy-done.7), custom_call_target="tpu_custom_call" | custom-call | tf_op jit(solution)/shard_map/pallas_call | solution.py:234
  28.9 27.1 %all_to_all.20 = bf16[16,32,1280]{2,1,0:T(8,128)(2,1)S(1)} all-to-all(bf16[16,32,1280]{2,1,0:T(8,128)(2,1)} %bitcast.30), channel_id=1, replica_groups=mesh['z'=4,'x'=4,'m'=2,'y0'=2,'c'=2] {'z','x'}, dimensions={0} | all-to-all | bytes 2621440 | tf_op jit(solution)/shard_map/all_to_all | solution.py:273
  56.5 36.4 %all_to_all.21 = bf16[32,32,1280]{2,1,0:T(8,128)(2,1)S(1)} all-to-all(bf16[32,32,1280]{2,1,0:T(8,128)(2,1)S(1)} %broadcast_in_dim.4), channel_id=1, replica_groups=mesh['z'=4,'x'=4,'m'=2,'y0'=2,'c'=2] {'y0','z','x'}, dimensions={0} | all-to-all | bytes 5242880 | tf_op jit(solution)/shard_map/all_to_all | solution.py:43
  92.9 2.8 %collective-permute-start.4 = (bf16[1024,1280]{1,0:T(8,128)(2,1)S(1)}, bf16[1024,1280]{1,0:T(8,128)(2,1)}, u32[]{:S(2)}, u32[]{:S(2)}) collective-permute-start(bf16[1024,1280]{1,0:T(8,128)(2,1)S(1)} %bitcast.24), channel_id=1, source_target_pairs={{0,1},{1,0},{2,3},{3,2},{4,5},{5,4},{6,7},{7,6},{8,9},{9,8},{10,11... | collective-permute-start | bytes 7864328 | tf_op jit(solution)/shard_map/ppermute | solution.py:47
  96.3 4.1 %collective-permute-done.4.other = bf16[1024,1280]{1,0:T(8,128)(2,1)} collective-permute-done((bf16[1024,1280]{1,0:T(8,128)(2,1)S(1)}, bf16[1024,1280]{1,0:T(8,128)(2,1)}, u32[]{:S(2)}, u32[]{:S(2)}) %collective-permute-start.4) | collective-permute-done | bytes 2621472 | tf_op jit(solution)/shard_map/ppermute | solution.py:47
  100.4 13.2 %shard_map.59 = (bf16[32,1280]{1,0:T(8,128)(2,1)}, f32[88,2048]{1,0:T(8,128)}) custom-call(s32[2]{0:T(128)} %pad_add_fusion.where, bf16[1024,1280]{1,0:T(8,128)(2,1)} %bitcast.25, bf16[1024,1280]{1,0:T(8,128)(2,1)} %collective-permute-done.4.other, bf16[88,2048]{1,0:T(8,128)(2,1)} %get-tuple-element.8.plain), custom_call_target="tpu_custom_call" | custom-call | tf_op jit(solution)/shard_map/pallas_call | solution.py:234
  113.6 1.2 broadcast_in_dim.5
  114.8 36.7 %all_to_all.22 = bf16[32,32,1280]{2,1,0:T(8,128)(2,1)S(1)} all-to-all(bf16[32,32,1280]{2,1,0:T(8,128)(2,1)S(1)} %broadcast_in_dim.5), channel_id=1, replica_groups=mesh['z'=4,'x'=4,'m'=2,'y0'=2,'c'=2] {'y0','z','x'}, dimensions={0} | all-to-all | bytes 5242880 | tf_op jit(solution)/shard_map/all_to_all | solution.py:43
  151.5 1.9 collective-permute-start.5
  153.4 4.5 %collective-permute-done.5.other = bf16[1024,1280]{1,0:T(8,128)(2,1)S(1)} collective-permute-done((bf16[1024,1280]{1,0:T(8,128)(2,1)S(1)}, bf16[1024,1280]{1,0:T(8,128)(2,1)S(1)}, u32[]{:S(2)}, u32[]{:S(2)}) %collective-permute-start.5) | collective-permute-done | bytes 2621472 | tf_op jit(solution)/shard_map/ppermute | solution.py:47
  158.0 1.5 copy-done.2
  159.5 30.6 %shard_map.60 = bf16[88,2048]{1,0:T(8,128)(2,1)} custom-call(s32[2]{0:T(128)} %pad_add_fusion.where, bf16[1024,1280]{1,0:T(8,128)(2,1)} %bitcast.23, bf16[1024,1280]{1,0:T(8,128)(2,1)} %copy-done.2, f32[88,2048]{1,0:T(8,128)} %get-tuple-element.10.x1), custom_call_target="tpu_custom_call" | custom-call | tf_op jit(solution)/shard_map/pallas_call | solution.py:234
  190.1 1.1 copy.10
  191.2 8.9 %all_to_all.23 = bf16[4,88,512]{2,1,0:T(8,128)(2,1)S(1)} all-to-all(bf16[4,88,512]{2,1,0:T(8,128)(2,1)S(1)} %bitcast.28), channel_id=1, replica_groups=mesh['z'=4,'x'=4,'m'=2,'y0'=2,'c'=2] {'c','y0'}, dimensions={0} | all-to-all | bytes 720896 | tf_op jit(solution)/shard_map/all_to_all | solution.py:306
  200.1 2.7 %collective-permute-start.6 = (bf16[352,256]{1,0:T(8,128)(2,1)S(1)}, bf16[352,256]{1,0:T(8,128)(2,1)S(1)}, u32[]{:S(2)}, u32[]{:S(2)}) collective-permute-start(bf16[352,256]{1,0:T(8,128)(2,1)S(1)} %slice.21), channel_id=1, source_target_pairs={{0,4},{4,0},{1,5},{5,1},{2,6},{6,2},{3,7},{7,3},{8,12},{12,8},{9,1... | collective-permute-start | bytes 540680 | tf_op jit(solution)/shard_map/ppermute | solution.py:47
  202.8 4.1 %collective-permute-done.6 = bf16[352,256]{1,0:T(8,128)(2,1)S(1)} collective-permute-done((bf16[352,256]{1,0:T(8,128)(2,1)S(1)}, bf16[352,256]{1,0:T(8,128)(2,1)S(1)}, u32[]{:S(2)}, u32[]{:S(2)}) %collective-permute-start.6) | collective-permute-done | bytes 180256 | tf_op jit(solution)/shard_map/ppermute | solution.py:47
  206.9 1.3 convert_multiply_fusion
  (25 shorter events, 3.3 us)
Async XLA Ops:
  3.0 7.8 %collective-permute-start = (bf16[352,256]{1,0:T(8,128)(2,1)S(1)}, bf16[352,256]{1,0:T(8,128)(2,1)S(1)}, u32[]{:S(2)}, u32[]{:S(2)}) collective-permute-start(bf16[352,256]{1,0:T(8,128)(2,1)S(1)} %get-tuple-element.18), channel_id=1, source_target_pairs={{0,4},{4,0},{1,5},{5,1},{2,6},{6,2},{3,7},{7,3},{8,12},{12,8},{9,1... | collective-permute-start | bytes 540680 | tf_op jit(solution)/shard_map/ppermute | solution.py:47
  10.9 12.2 %copy-start.3 = (bf16[352,512]{1,0:T(8,128)(2,1)}, bf16[352,512]{1,0:T(8,128)(2,1)S(1)}, u32[]{:S(2)}) copy-start(bf16[352,512]{1,0:T(8,128)(2,1)S(1)} %pad_maximum_fusion.b0) | copy-start | bytes 1081348
  10.9 8.6 %collective-permute-start.1 = (bf16[352,512]{1,0:T(8,128)(2,1)S(1)}, bf16[352,512]{1,0:T(8,128)(2,1)S(1)}, u32[]{:S(2)}, u32[]{:S(2)}) collective-permute-start(bf16[352,512]{1,0:T(8,128)(2,1)S(1)} %pad_maximum_fusion.b0), channel_id=1, source_target_pairs={{0,2},{2,0},{1,3},{3,1},{4,6},{6,4},{5,7},{7,5},{8,10},{10,8},{9,1... | collective-permute-start | bytes 1081352 | tf_op jit(solution)/shard_map/ppermute | solution.py:47
  12.2 10.2 %collective-permute-start.2 = (bf16[352,512]{1,0:T(8,128)(2,1)S(1)}, bf16[352,512]{1,0:T(8,128)(2,1)S(1)}, u32[]{:S(2)}, u32[]{:S(2)}) collective-permute-start(bf16[352,512]{1,0:T(8,128)(2,1)S(1)} %pad_maximum_fusion.b0), channel_id=1, source_target_pairs={{0,1},{1,0},{2,3},{3,2},{4,5},{5,4},{6,7},{7,6},{8,9},{9,8},{10,11... | collective-permute-start | bytes 1081352 | tf_op jit(solution)/shard_map/ppermute | solution.py:47
  19.5 3.6 %copy-start.5 = (bf16[352,512]{1,0:T(8,128)(2,1)}, bf16[352,512]{1,0:T(8,128)(2,1)S(1)}, u32[]{:S(2)}) copy-start(bf16[352,512]{1,0:T(8,128)(2,1)S(1)} %collective-permute-done.1.b1) | copy-start | bytes 1081348
  19.5 3.6 %collective-permute-start.3 = (bf16[352,512]{1,0:T(8,128)(2,1)S(1)}, bf16[352,512]{1,0:T(8,128)(2,1)S(1)}, u32[]{:S(2)}, u32[]{:S(2)}) collective-permute-start(bf16[352,512]{1,0:T(8,128)(2,1)S(1)} %collective-permute-done.1.b1), channel_id=1, source_target_pairs={{0,1},{1,0},{2,3},{3,2},{4,5},{5,4},{6,7},{7,6},{8,9},{9,8},{10,11... | collective-permute-start | bytes 1081352 | tf_op jit(solution)/shard_map/ppermute | solution.py:47
  22.4 0.7 copy-start.6
  23.1 0.7 copy-start.7
  92.9 7.5 %copy-start.1 = (bf16[32,32,1280]{2,1,0:T(8,128)(2,1)}, bf16[32,32,1280]{2,1,0:T(8,128)(2,1)S(1)}, u32[]{:S(2)}) copy-start(bf16[32,32,1280]{2,1,0:T(8,128)(2,1)S(1)} %all_to_all.21) | copy-start | bytes 7864324
  92.9 7.5 %collective-permute-start.4 = (bf16[1024,1280]{1,0:T(8,128)(2,1)S(1)}, bf16[1024,1280]{1,0:T(8,128)(2,1)}, u32[]{:S(2)}, u32[]{:S(2)}) collective-permute-start(bf16[1024,1280]{1,0:T(8,128)(2,1)S(1)} %bitcast.24), channel_id=1, source_target_pairs={{0,1},{1,0},{2,3},{3,2},{4,5},{5,4},{6,7},{7,6},{8,9},{9,8},{10,11... | collective-permute-start | bytes 7864328 | tf_op jit(solution)/shard_map/ppermute | solution.py:47
  151.5 8.0 %copy-start = (bf16[32,32,1280]{2,1,0:T(8,128)(2,1)}, bf16[32,32,1280]{2,1,0:T(8,128)(2,1)S(1)}, u32[]{:S(2)}) copy-start(bf16[32,32,1280]{2,1,0:T(8,128)(2,1)S(1)} %all_to_all.22) | copy-start | bytes 7864324
  151.5 6.5 %collective-permute-start.5 = (bf16[1024,1280]{1,0:T(8,128)(2,1)S(1)}, bf16[1024,1280]{1,0:T(8,128)(2,1)S(1)}, u32[]{:S(2)}, u32[]{:S(2)}) collective-permute-start(bf16[1024,1280]{1,0:T(8,128)(2,1)S(1)} %bitcast.22), channel_id=1, source_target_pairs={{0,1},{1,0},{2,3},{3,2},{4,5},{5,4},{6,7},{7,6},{8,9},{9,8},{10,11... | collective-permute-start | bytes 7864328 | tf_op jit(solution)/shard_map/ppermute | solution.py:47
  158.0 1.5 copy-start.2
  190.1 16.8 %copy-start.4 = (f32[2,352,256]{2,1,0:T(8,128)S(1)}, f32[2,352,256]{2,1,0:T(8,128)}, u32[]{:S(2)}) copy-start(f32[2,352,256]{2,1,0:T(8,128)} %param.3) | copy-start | bytes 2162692
  200.1 6.8 %collective-permute-start.6 = (bf16[352,256]{1,0:T(8,128)(2,1)S(1)}, bf16[352,256]{1,0:T(8,128)(2,1)S(1)}, u32[]{:S(2)}, u32[]{:S(2)}) collective-permute-start(bf16[352,256]{1,0:T(8,128)(2,1)S(1)} %slice.21), channel_id=1, source_target_pairs={{0,4},{4,0},{1,5},{5,1},{2,6},{6,2},{3,7},{7,3},{8,12},{12,8},{9,1... | collective-permute-start | bytes 540680 | tf_op jit(solution)/shard_map/ppermute | solution.py:47

commit v3 on v0

v3 whole, which is shorter than its diff:
```python
import math

import jax
import jax.numpy as jnp
from jax import lax
from jax.experimental import pallas as pl
from jax.experimental.pallas import tpu as pltpu
from jax.sharding import Mesh, PartitionSpec as P

D = 2048
FF = 5632

MOMENTUM_DECAY = 0.95
A1 = 3.4445
A2 = -4.775
A3 = 2.0315
LEARN_RATE = 0.02
WEIGHT_DECAY = 0.1
EPSILON = 1e-07
STEP_SCALE = 0.2
NORM_SAFETY = 1.8

SHIFT = -A2 / (2.0 * A3)
REST = A1 - A3 * SHIFT * SHIFT

BF = jnp.bfloat16
F32 = jnp.float32

ROWS = 88
GROWS = 32
BLK = 128
PANELS = 16
PACK = 9 * BLK
WIDE = 256
TILE = 512

VMEM = pl.BlockSpec(memory_space=pltpu.VMEM)


def at(start, size, align=None):
    return pl.ds(pl.multiple_of(start, align or size), size)


def swap(value, axis):
    return lax.ppermute(value, axis, [(0, 1), (1, 0)])


def unpack(full, own, other, core):
    for part, base in ((own, core * 8), (other, (1 - core) * 8)):

        def panel(k, carry, part=part, base=base):
            here = base + k
            rows = at(k * BLK, BLK)
            for d in range(9):
                there = lax.rem(here + d, PANELS)
                block = part[rows, d * BLK : (d + 1) * BLK]
                full[at(here * BLK, BLK), at(there * BLK, BLK)] = block
                if 0 < d < 8:
                    full[at(there * BLK, BLK), at(here * BLK, BLK)] = block.T
            return carry

        lax.fori_loop(0, 8, panel, 0)


def square_sum(parts):
    total = jnp.zeros((1, BLK), F32)
    for part in parts:

        def panel(k, total, part=part):
            for d in range(9):
                block = part[at(k * BLK, BLK), d * BLK : (d + 1) * BLK].astype(F32)
                value = jnp.sum(block * block, axis=0, keepdims=True)
                total = total + (2.0 * value if 0 < d < 8 else value)
            return total

        total = lax.fori_loop(0, 8, panel, total)
    return jnp.sum(total, axis=1, keepdims=True)


def columns(body):
    def step(n, carry):
        body(n, at(n * TILE, TILE))
        return carry

    lax.fori_loop(0, D // TILE, step, 0)


def dot(left, right):
    return jnp.dot(left, right, preferred_element_type=F32)


def gram_kernel(near, far, out, rows_out, whole):
    core, half = lax.axis_index("c"), lax.axis_index("y0")
    slot = core * 2 + half
    for k in range(4):
        whole[:, at((core * 4 + k) * WIDE, WIDE)] = near[k]
        whole[:, at(((1 - core) * 4 + k) * WIDE, WIDE)] = far[k]
    whole[:, D:] = whole[:, : PACK - BLK]
    for j in range(2):
        left = near[2 * half + j].T
        for i in range(2):
            start = slot * TILE + j * WIDE + i * BLK
            value = dot(left[i * BLK : (i + 1) * BLK], whole[:, at(start, PACK, BLK)])
            out[(2 * j + i) * BLK : (2 * j + i + 1) * BLK, :] = value.astype(BF)
    for k in range(4):

        @pl.when(slot == k)
        def _(k=k):
            rows_out[...] = whole[k * ROWS : (k + 1) * ROWS, :D]


def first_kernel(own, other, plain, rows_out, x_out, full, l1, l2, u, hold, w, g1):
    core = lax.axis_index("c")
    index = lax.axis_index("y0") * 16 + lax.axis_index("z") * 4 + lax.axis_index("x")
    row = core * (D // 2) + index * GROWS
    unpack(full, own, other, core)
    squares = square_sum((own, other))
    ratio = 1.0 / (NORM_SAFETY * jnp.sqrt(jnp.sqrt(squares / D)) + EPSILON)
    q = ratio * ratio
    l1[:GROWS, :] = full[at(row, GROWS), :]
    l1[GROWS:, :] = plain[...]

    def one(n, sl):
        value = q * dot(l1[...], full[:, sl]) - SHIFT * l1[:, sl].astype(F32)
        u[:, sl] = value
        l2[:, sl] = value.astype(BF)

    columns(one)

    def two(n, sl):
        value = q * dot(l2[...], full[:, sl])
        mixed = REST * l1[:, sl].astype(F32) + A3 * (value - SHIFT * u[:, sl])
        x_out[:, sl] = ratio * mixed[GROWS:]
        hold[:, sl] = q * mixed[:GROWS]

    columns(two)
    l1[:GROWS, :] = hold[...].astype(BF)

    def three(n, sl):
        value = q * dot(l1[:GROWS, :], full[:, sl]) - SHIFT * hold[:, sl]
        w[:, sl] = value
        l2[:GROWS, sl] = value.astype(BF)

    columns(three)

    def four(n, sl):
        value = q * dot(l2[:GROWS, :], full[:, sl])
        g1[:, sl] = (REST * hold[:, sl] + A3 * (value - SHIFT * w[:, sl])).astype(BF)

    columns(four)
    here = row // BLK
    packed = jnp.concatenate(
        [g1[:, at(lax.rem(here + d, PANELS) * BLK, BLK)] for d in range(9)], 1
    )

    def spread(i, carry):
        rows_out[i] = packed
        return carry

    lax.fori_loop(0, 32, spread, 0)


def second_kernel(own, other, x1, out, full, la, lb, x2, t, y, z):
    unpack(full, own, other, lax.axis_index("c"))
    lefts = [la, lb]

    def times(finish):
        src, dst = lefts

        def body(n, sl):
            value = finish(sl, dot(src[...], full[:, sl]))
            dst[:, sl] = value.astype(BF)

        columns(body)
        lefts.reverse()

    def keep(sl, value):
        t[:, sl] = value
        return value

    def less(base):
        def finish(sl, value):
            value = value - SHIFT * base[:, sl]
            y[:, sl] = value
            return value

        return finish

    def close(base, ref):
        def finish(sl, value):
            value = REST * base[:, sl] + A3 * (value - SHIFT * y[:, sl])
            ref[:, sl] = value
            return value

        return finish

    def middle(sl, value):
        value = REST * t[:, sl] + A3 * (value - SHIFT * y[:, sl]) - SHIFT * x2[:, sl]
        z[:, sl] = value
        return value

    la[...] = x1[...].astype(BF)
    times(less(x1))
    times(close(x1, x2))
    times(keep)
    times(less(t))
    times(close(t, t))
    times(less(t))
    times(middle)
    times(keep)
    times(less(t))
    times(close(t, t))
    times(less(t))
    src = lefts[0]

    def last(n, sl):
        value = REST * t[:, sl] + A3 * (dot(src[...], full[:, sl]) - SHIFT * y[:, sl])
        value = (REST * x2[:, sl] + A3 * (value - SHIFT * z[:, sl])).astype(BF)
        out[2 * n] = value[:, :WIDE]
        out[2 * n + 1] = value[:, WIDE:]

    columns(last)


def call(kernel, outs, scratch, *args):
    return pl.pallas_call(
        kernel,
        out_shape=outs,
        in_specs=[VMEM] * len(args),
        out_specs=[VMEM] * len(outs),
        scratch_shapes=scratch,
        compiler_params=pltpu.CompilerParams(vmem_limit_bytes=60 * 1024 * 1024),
    )(*args)


def shape(dims, dtype):
    return jax.ShapeDtypeStruct(dims, dtype)


def exchange(value, axes):
    return lax.all_to_all(value, axes, split_axis=0, concat_axis=0)


def per_device(weights, momentum, gradients):
    new_momentum = MOMENTUM_DECAY * momentum + gradients
    iterate = gradients + MOMENTUM_DECAY * new_momentum
    plain = iterate.astype(BF)

    near = exchange(jnp.stack([plain[0], plain[0], plain[1], plain[1]]), ("m", "y0"))
    far = swap(near, "c")
    partial, own_rows = call(
        gram_kernel,
        (shape((TILE, PACK), BF), shape((ROWS, D), BF)),
        [pltpu.VMEM((352, D + PACK - BLK), BF)],
        near, far,
    )
    pieces = exchange(partial.reshape(16, GROWS, PACK), ("z", "x"))
    gram_rows = jnp.sum(pieces.astype(F32), axis=0).astype(BF)

    def whole(spread):
        part = exchange(spread, ("y0", "z", "x")).reshape(D // 2, PACK)
        return part, swap(part, "c")

    own, away = whole(jnp.broadcast_to(gram_rows[None], (32, GROWS, PACK)))
    spread, x1 = call(
        first_kernel,
        (shape((32, GROWS, PACK), BF), shape((ROWS, D), F32)),
        [
            pltpu.VMEM((D, D), BF),
            pltpu.VMEM((GROWS + ROWS, D), BF),
            pltpu.VMEM((GROWS + ROWS, D), BF),
            pltpu.VMEM((GROWS + ROWS, D), F32),
            pltpu.VMEM((GROWS, D), F32),
            pltpu.VMEM((GROWS, D), F32),
            pltpu.VMEM((GROWS, D), BF),
        ],
        own, away, own_rows,
    )
    own, away = whole(spread)
    (x3,) = call(
        second_kernel,
        (shape((8, ROWS, WIDE), BF),),
        [pltpu.VMEM((D, D), BF)]
        + [pltpu.VMEM((ROWS, D), BF)] * 2
        + [pltpu.VMEM((ROWS, D), F32)] * 4,
        own, away, x1,
    )

    back = exchange(x3, ("c", "m", "y0")).reshape(2, 2, 2, ROWS, WIDE)
    both = back.transpose(1, 0, 2, 3, 4).reshape(2, 352, WIDE)

    update = STEP_SCALE * math.sqrt(max(FF, D)) * both.astype(F32)
    new_weights = weights * (1.0 - LEARN_RATE * WEIGHT_DECAY) - LEARN_RATE * update
    return (new_weights, new_momentum, update)


def solution(mesh):
    fine = Mesh(mesh.devices.reshape(4, 4, 2, 2, 2), ("z", "x", "m", "y0", "c"))
    spec = P(None, ("z", "x"), ("m", "y0", "c"))
    return jax.shard_map(
        per_device, mesh=fine, in_specs=(spec, spec, spec), out_specs=(spec, spec, spec), check_vma=False
    )
```

time: 568 us -> 195 us (0.34)
  waiting for transfers between devices: 294 us -> 10.1 us
  blocking collectives: 214 us -> 120 us
  Pallas kernels: 0 us -> 48.6 us
  matrix products: 39.3 us -> 0 us
  between operations: 14.2 us -> 0.68 us
  starting transfers between devices: 0.29 us -> 6.81 us
    psum x3 -> x0, blocking collectives: 214 us -> none  [the longest x2 201 us: per_device(): gram_rows = lax.psum(partial_value, 'fs')]
    all_gather x6 -> x0, waiting for transfers between devices: 190 us -> none  [the longest x3 96.3 us: per_device(): row_whole = lax.all_gather(plain, 'tp', axis=2, tiled=True)]
    all_to_all x0 -> x5, blocking collectives: none -> 120 us  [exchange(): return lax.all_to_all(value, axes, split_axis=0, concat_axis=0)]
    psum x1 -> x0, waiting for transfers between devices: 104 us -> none  [per_device(): gram_rows = lax.psum(partial_value, 'fs')]
    pallas_call x0 -> x3, Pallas kernels: none -> 48.6 us  [call(): pl.pallas_call(kernel, out_shape=outs, in_specs=[VMEM] * len(args), out_s...]
    dot_general x9 -> x0, matrix products: 39.3 us -> none  [the longest x3 15.6 us: per_device(): jnp.einsum('prj,prk->pjk', plain, row_whole, preferred_element_type=jnp.f...]
    ppermute x0 -> x3, waiting for transfers between devices: none -> 10.1 us  [swap(): return lax.ppermute(value, axis, [(0, 1), (1, 0)])]
    ppermute x0 -> x3, starting transfers between devices: none -> 6.81 us  [swap(): return lax.ppermute(value, axis, [(0, 1), (1, 0)])]
  transfers between devices with their start and end apart: 7 -> 3, of which waited for: 7 -> 3; matrix products, arithmetic and copies ran while one was open for 0% -> 0% of each run, Pallas kernels for 0% -> 0%
where the time goes in v3:
time: 195 us
  blocking collectives  120 us (62%)
  Pallas kernels  48.6 us (25%)
  waiting for transfers between devices  10.1 us (5%)
  starting transfers between devices  6.81 us (3%)
  local copies, waits for them, and re-layouts  4.89 us (3%)
  other arithmetic  3.64 us (2%)
    all_to_all x5, blocking collectives, exchange(): return lax.all_to_all(value, axes, split_axis=0, concat_axis=0)  120 us
    pallas_call x3, Pallas kernels, call(): pl.pallas_call(kernel, out_shape=outs, in_specs=[VMEM] * len(args), out_s...  48.6 us
    ppermute x3, waiting for transfers between devices, swap(): return lax.ppermute(value, axis, [(0, 1), (1, 0)])  10.1 us
    ppermute x3, starting transfers between devices, swap(): return lax.ppermute(value, axis, [(0, 1), (1, 0)])  6.81 us
  transfers between devices with their start and end apart: 3, of which 3 were waited for; matrix products, arithmetic and copies ran while one was open for 0% of the time, Pallas kernels for 0%

profile of v3, /device:TPU:1, one launch (start us, length us, event | category | flops | bytes accessed | tf_op | source)
XLA Modules:
  0.0 194.6 jit_solution(5735994016756434869)
XLA Ops:
  0.6 2.3 %add_convert_fusion = (bf16[2,352,256]{2,1,0:T(8,128)(2,1)S(1)}, f32[2,352,256]{2,1,0:T(8,128)}) fusion(f32[2,352,256]{2,1,0:T(8,128)} %param.5, f32[2,352,256]{2,1,0:T(8,128)} %param.4), kind=kLoop, calls=%fused_computation.4 | loop fusion | flops 901120 | bytes 2523136 | tf_op jit(solution)/shard_map/convert_element_type | solution.py:247
  3.0 0.1 pad_maximum_fusion
  3.1 15.2 %all_to_all.25.near = bf16[4,352,256]{2,1,0:T(8,128)(2,1)S(1)} all-to-all(bf16[4,352,256]{2,1,0:T(8,128)(2,1)S(1)} %pad_maximum_fusion), channel_id=1, replica_groups=mesh['z'=4,'x'=4,'m'=2,'y0'=2,'c'=2] {'m','y0'}, dimensions={0} | all-to-all | bytes 1441792 | tf_op jit(solution)/shard_map/all_to_all | solution.py:241
  18.3 2.1 %collective-permute-start = (bf16[4,352,256]{2,1,0:T(8,128)(2,1)S(1)}, bf16[4,352,256]{2,1,0:T(8,128)(2,1)S(1)}, u32[]{:S(2)}, u32[]{:S(2)}) collective-permute-start(bf16[4,352,256]{2,1,0:T(8,128)(2,1)S(1)} %all_to_all.25.near), channel_id=1, source_target_pairs={{0,1},{1,0},{2,3},{3,2},{4,5},{5,4},{6,7},{7,6},{8,9},{9,8},{10,11... | collective-permute-start | bytes 2162696 | tf_op jit(solution)/shard_map/ppermute | solution.py:45
  20.4 1.8 collective-permute-done.far
  22.2 0.9 copy-done.6
  23.1 3.7 %shard_map.58 = (bf16[512,1152]{1,0:T(8,128)(2,1)}, bf16[88,2048]{1,0:T(8,128)(2,1)}) custom-call(bf16[4,352,256]{2,1,0:T(8,128)(2,1)} %copy-done.2, bf16[4,352,256]{2,1,0:T(8,128)(2,1)} %copy-done.6), custom_call_target="tpu_custom_call" | custom-call | tf_op jit(solution)/shard_map/pallas_call | solution.py:226
  26.8 25.7 %all_to_all.26 = bf16[16,32,1152]{2,1,0:T(8,128)(2,1)S(1)} all-to-all(bf16[16,32,1152]{2,1,0:T(8,128)(2,1)} %bitcast.18), channel_id=1, replica_groups=mesh['z'=4,'x'=4,'m'=2,'y0'=2,'c'=2] {'z','x'}, dimensions={0} | all-to-all | bytes 2359296 | tf_op jit(solution)/shard_map/all_to_all | solution.py:241
  52.5 0.2 reduce_sum.12
  52.7 0.2 broadcast_in_dim.2
  52.8 33.1 %all_to_all.27 = bf16[32,32,1152]{2,1,0:T(8,128)(2,1)S(1)} all-to-all(bf16[32,32,1152]{2,1,0:T(8,128)(2,1)S(1)} %broadcast_in_dim.2), channel_id=1, replica_groups=mesh['z'=4,'x'=4,'m'=2,'y0'=2,'c'=2] {'y0','z','x'}, dimensions={0} | all-to-all | bytes 4718592 | tf_op jit(solution)/shard_map/all_to_all | solution.py:241
  86.0 2.6 %collective-permute-start.1 = (bf16[1024,1152]{1,0:T(8,128)(2,1)S(1)}, bf16[1024,1152]{1,0:T(8,128)(2,1)S(1)}, u32[]{:S(2)}, u32[]{:S(2)}) collective-permute-start(bf16[1024,1152]{1,0:T(8,128)(2,1)S(1)} %bitcast.12), channel_id=1, source_target_pairs={{0,1},{1,0},{2,3},{3,2},{4,5},{5,4},{6,7},{7,6},{8,9},{9,8},{10,11... | collective-permute-start | bytes 7077896 | tf_op jit(solution)/shard_map/ppermute | solution.py:45
  88.6 4.2 %collective-permute-done.1.other = bf16[1024,1152]{1,0:T(8,128)(2,1)S(1)} collective-permute-done((bf16[1024,1152]{1,0:T(8,128)(2,1)S(1)}, bf16[1024,1152]{1,0:T(8,128)(2,1)S(1)}, u32[]{:S(2)}, u32[]{:S(2)}) %collective-permute-start.1) | collective-permute-done | bytes 2359328 | tf_op jit(solution)/shard_map/ppermute | solution.py:45
  92.8 1.4 copy-done.3
  94.2 15.9 %shard_map.59 = (bf16[32,32,1152]{2,1,0:T(8,128)(2,1)}, f32[88,2048]{1,0:T(8,128)}) custom-call(bf16[1024,1152]{1,0:T(8,128)(2,1)} %bitcast.13, bf16[1024,1152]{1,0:T(8,128)(2,1)} %copy-done.3, bf16[88,2048]{1,0:T(8,128)(2,1)} %get-tuple-element.8.plain), custom_call_target="tpu_custom_call" | custom-call | tf_op jit(solution)/shard_map/pallas_call | solution.py:226
  110.1 34.3 %all_to_all.28 = bf16[32,32,1152]{2,1,0:T(8,128)(2,1)S(1)} all-to-all(bf16[32,32,1152]{2,1,0:T(8,128)(2,1)} %get-tuple-element.9), channel_id=1, replica_groups=mesh['z'=4,'x'=4,'m'=2,'y0'=2,'c'=2] {'y0','z','x'}, dimensions={0} | all-to-all | bytes 4718592 | tf_op jit(solution)/shard_map/all_to_all | solution.py:241
  144.4 2.1 %collective-permute-start.2 = (bf16[1024,1152]{1,0:T(8,128)(2,1)S(1)}, bf16[1024,1152]{1,0:T(8,128)(2,1)S(1)}, u32[]{:S(2)}, u32[]{:S(2)}) collective-permute-start(bf16[1024,1152]{1,0:T(8,128)(2,1)S(1)} %bitcast.14), channel_id=1, source_target_pairs={{0,1},{1,0},{2,3},{3,2},{4,5},{5,4},{6,7},{7,6},{8,9},{9,8},{10,11... | collective-permute-start | bytes 7077896 | tf_op jit(solution)/shard_map/ppermute | solution.py:45
  146.4 4.2 %collective-permute-done.2.other = bf16[1024,1152]{1,0:T(8,128)(2,1)S(1)} collective-permute-done((bf16[1024,1152]{1,0:T(8,128)(2,1)S(1)}, bf16[1024,1152]{1,0:T(8,128)(2,1)S(1)}, u32[]{:S(2)}, u32[]{:S(2)}) %collective-permute-start.2) | collective-permute-done | bytes 2359328 | tf_op jit(solution)/shard_map/ppermute | solution.py:45
  150.6 1.4 copy-done.4
  152.0 29.0 %shard_map.60 = bf16[8,88,256]{2,1,0:T(8,128)(2,1)} custom-call(bf16[1024,1152]{1,0:T(8,128)(2,1)} %bitcast.15, bf16[1024,1152]{1,0:T(8,128)(2,1)} %copy-done.4, f32[88,2048]{1,0:T(8,128)} %get-tuple-element.10.x1), custom_call_target="tpu_custom_call" | custom-call | tf_op jit(solution)/shard_map/pallas_call | solution.py:226
  181.0 11.5 %all_to_all.29 = bf16[8,88,256]{2,1,0:T(8,128)(2,1)S(1)} all-to-all(bf16[8,88,256]{2,1,0:T(8,128)(2,1)} %shard_map.60), channel_id=1, replica_groups=mesh['z'=4,'x'=4,'m'=2,'y0'=2,'c'=2] {'c','m','y0'}, dimensions={0} | all-to-all | bytes 720896 | tf_op jit(solution)/shard_map/all_to_all | solution.py:241
  192.5 0.1 convert_multiply_fusion
  192.6 0.9 copy.7
  193.6 1.0 bitcast_subtract_fusion
  (13 shorter events, 0.1 us)
Async XLA Ops:
  18.3 3.9 %copy-start.2 = (bf16[4,352,256]{2,1,0:T(8,128)(2,1)}, bf16[4,352,256]{2,1,0:T(8,128)(2,1)S(1)}, u32[]{:S(2)}) copy-start(bf16[4,352,256]{2,1,0:T(8,128)(2,1)S(1)} %all_to_all.25.near) | copy-start | bytes 2162692
  18.3 3.9 %collective-permute-start = (bf16[4,352,256]{2,1,0:T(8,128)(2,1)S(1)}, bf16[4,352,256]{2,1,0:T(8,128)(2,1)S(1)}, u32[]{:S(2)}, u32[]{:S(2)}) collective-permute-start(bf16[4,352,256]{2,1,0:T(8,128)(2,1)S(1)} %all_to_all.25.near), channel_id=1, source_target_pairs={{0,1},{1,0},{2,3},{3,2},{4,5},{5,4},{6,7},{7,6},{8,9},{9,8},{10,11... | collective-permute-start | bytes 2162696 | tf_op jit(solution)/shard_map/ppermute | solution.py:45
  22.2 0.9 copy-start.6
  86.0 8.2 %copy-start = (bf16[32,32,1152]{2,1,0:T(8,128)(2,1)}, bf16[32,32,1152]{2,1,0:T(8,128)(2,1)S(1)}, u32[]{:S(2)}) copy-start(bf16[32,32,1152]{2,1,0:T(8,128)(2,1)S(1)} %all_to_all.27) | copy-start | bytes 7077892
  86.0 6.8 %collective-permute-start.1 = (bf16[1024,1152]{1,0:T(8,128)(2,1)S(1)}, bf16[1024,1152]{1,0:T(8,128)(2,1)S(1)}, u32[]{:S(2)}, u32[]{:S(2)}) collective-permute-start(bf16[1024,1152]{1,0:T(8,128)(2,1)S(1)} %bitcast.12), channel_id=1, source_target_pairs={{0,1},{1,0},{2,3},{3,2},{4,5},{5,4},{6,7},{7,6},{8,9},{9,8},{10,11... | collective-permute-start | bytes 7077896 | tf_op jit(solution)/shard_map/ppermute | solution.py:45
  92.8 1.4 copy-start.3
  144.4 7.6 %copy-start.1 = (bf16[32,32,1152]{2,1,0:T(8,128)(2,1)}, bf16[32,32,1152]{2,1,0:T(8,128)(2,1)S(1)}, u32[]{:S(2)}) copy-start(bf16[32,32,1152]{2,1,0:T(8,128)(2,1)S(1)} %all_to_all.28) | copy-start | bytes 7077892
  144.4 6.2 %collective-permute-start.2 = (bf16[1024,1152]{1,0:T(8,128)(2,1)S(1)}, bf16[1024,1152]{1,0:T(8,128)(2,1)S(1)}, u32[]{:S(2)}, u32[]{:S(2)}) collective-permute-start(bf16[1024,1152]{1,0:T(8,128)(2,1)S(1)} %bitcast.14), channel_id=1, source_target_pairs={{0,1},{1,0},{2,3},{3,2},{4,5},{5,4},{6,7},{7,6},{8,9},{9,8},{10,11... | collective-permute-start | bytes 7077896 | tf_op jit(solution)/shard_map/ppermute | solution.py:45
  150.6 1.4 copy-start.4
  192.5 1.2 copy-start.5

commit v4 on v3

v4 whole, which is shorter than its diff:
```python
import math

import jax
import jax.numpy as jnp
from jax import lax
from jax.experimental import pallas as pl
from jax.experimental.pallas import tpu as pltpu
from jax.sharding import Mesh, PartitionSpec as P

D = 2048
FF = 5632

MOMENTUM_DECAY = 0.95
A1 = 3.4445
A2 = -4.775
A3 = 2.0315
LEARN_RATE = 0.02
WEIGHT_DECAY = 0.1
EPSILON = 1e-07
STEP_SCALE = 0.2
NORM_SAFETY = 1.8

SHIFT = -A2 / (2.0 * A3)
REST = A1 - A3 * SHIFT * SHIFT

BF = jnp.bfloat16
F32 = jnp.float32

ROWS = 88
GROWS = 32
BLK = 128
PANELS = 16
PACK = 9 * BLK
WIDE = 256
TILE = 512

VMEM = pl.BlockSpec(memory_space=pltpu.VMEM)


def at(start, size, align=None):
    return pl.ds(pl.multiple_of(start, align or size), size)


def swap(value, axis):
    return lax.ppermute(value, axis, [(0, 1), (1, 0)])


def unpack(full, own, other):
    for part, base in ((own, 0), (other, 8)):
        for k in range(8):
            here = base + k
            for d in range(9):
                there = (here + d) % PANELS
                block = part[k * BLK : (k + 1) * BLK, d * BLK : (d + 1) * BLK]
                full[here * BLK : (here + 1) * BLK, there * BLK : (there + 1) * BLK] = block
                if 0 < d < 8:
                    full[there * BLK : (there + 1) * BLK, here * BLK : (here + 1) * BLK] = block.T


def square_sum(parts):
    total = jnp.zeros((1, PACK), F32)
    for part in parts:

        def panel(k, total, part=part):
            block = part[at(k * BLK, BLK), :].astype(F32)
            return total + jnp.sum(block * block, axis=0, keepdims=True)

        total = lax.fori_loop(0, 8, panel, total)
    lane = lax.broadcasted_iota(jnp.int32, (1, PACK), 1)
    twice = jnp.logical_and(lane >= BLK, lane < 8 * BLK)
    return jnp.sum(jnp.where(twice, 2.0 * total, total), axis=1, keepdims=True)


def columns(body):
    for n in range(D // TILE):
        body(n, slice(n * TILE, (n + 1) * TILE))


def dot(left, right):
    return jnp.dot(left, right, preferred_element_type=F32)


def gram_kernel(near, far, out, rows_out, whole):
    core, half = lax.axis_index("c"), lax.axis_index("y0")
    for k in range(4):
        whole[:, k * WIDE : (k + 1) * WIDE] = near[k]
        whole[:, (4 + k) * WIDE : (5 + k) * WIDE] = far[k]
    for j in range(2):
        left = near[2 * half + j].T
        for i in range(2):
            start = half * TILE + j * WIDE + i * BLK
            value = dot(left[i * BLK : (i + 1) * BLK], whole[:, at(start, PACK, BLK)])
            out[(2 * j + i) * BLK : (2 * j + i + 1) * BLK, :] = value.astype(BF)
    for k in range(4):

        @pl.when(core * 2 + half == k)
        def _(k=k):
            rows_out[...] = whole[k * ROWS : (k + 1) * ROWS, :]


def first_kernel(own, other, plain, rows_out, x_out, full, l1, l2, u, hold, w, g1):
    row = (lax.axis_index("y0") * 16 + lax.axis_index("z") * 4 + lax.axis_index("x")) * GROWS
    unpack(full, own, other)
    squares = square_sum((own, other))
    ratio = 1.0 / (NORM_SAFETY * jnp.sqrt(jnp.sqrt(squares / D)) + EPSILON)
    q = ratio * ratio
    l1[:GROWS, :] = full[at(row, GROWS), :]
    l1[GROWS:, :] = plain[...]

    def one(n, sl):
        value = q * dot(l1[...], full[:, sl]) - SHIFT * l1[:, sl].astype(F32)
        u[:, sl] = value
        l2[:, sl] = value.astype(BF)

    columns(one)

    def two(n, sl):
        value = q * dot(l2[...], full[:, sl])
        mixed = REST * l1[:, sl].astype(F32) + A3 * (value - SHIFT * u[:, sl])
        x_out[:, sl] = ratio * mixed[GROWS:]
        hold[:, sl] = q * mixed[:GROWS]

    columns(two)
    l1[:GROWS, :] = hold[...].astype(BF)

    def three(n, sl):
        value = q * dot(l1[:GROWS, :], full[:, sl]) - SHIFT * hold[:, sl]
        w[:, sl] = value
        l2[:GROWS, sl] = value.astype(BF)

    columns(three)

    def four(n, sl):
        value = q * dot(l2[:GROWS, :], full[:, sl])
        g1[:, sl] = (REST * hold[:, sl] + A3 * (value - SHIFT * w[:, sl])).astype(BF)

    columns(four)
    packed = g1[:, at((row // BLK) * BLK, PACK, BLK)]

    def spread(i, carry):
        rows_out[i] = packed
        return carry

    lax.fori_loop(0, 32, spread, 0)


X1, X2, T, Y, Z = range(5)


def second_kernel(own, other, x1, out, full, left, buf):
    core = lax.axis_index("c")
    unpack(full, own, other)
    buf[X1] = x1[...]
    buf[T] = jnp.zeros((ROWS, D), F32)
    buf[Y] = jnp.zeros((ROWS, D), F32)
    left[0] = x1[...].astype(BF)

    def product(i, carry):
        keep = jnp.logical_or(i == 2, i == 7)
        less = (i == 0) | (i == 3) | (i == 5) | (i == 8) | (i == 10)
        scale = jnp.where(jnp.logical_or(keep, less), 1.0, A3)
        scale_base = jnp.where(keep, 0.0, jnp.where(less, -SHIFT, REST))
        scale_y = jnp.where(jnp.logical_or(keep, less), 0.0, -A3 * SHIFT)
        base = jnp.where(i < 2, X1, T)
        into = jnp.where(less, Y, jnp.where(i == 1, X2, jnp.where(i == 6, Z, T)))
        src = lax.rem(i, 2)
        for n in range(D // TILE):
            sl = slice(n * TILE, (n + 1) * TILE)
            value = scale * dot(left[src], full[:, sl])
            value = value + scale_base * buf[base, :, sl] + scale_y * buf[Y, :, sl]
            buf[into, :, sl] = value
            left[1 - src, :, sl] = value.astype(BF)

        @pl.when(i == 6)
        def _():
            value = buf[Z] - SHIFT * buf[X2]
            buf[Z] = value
            left[1 - src] = value.astype(BF)

        return carry

    lax.fori_loop(0, 11, product, 0)
    for n in range(D // TILE):
        sl = slice(n * TILE, (n + 1) * TILE)
        value = dot(left[1], full[:, sl]) - SHIFT * buf[Y, :, sl]
        value = REST * buf[T, :, sl] + A3 * value - SHIFT * buf[Z, :, sl]
        value = (REST * buf[X2, :, sl] + A3 * value).astype(BF)
        for k in range(2):
            out[lax.rem(2 * n + k + core * 4, 8)] = value[:, k * WIDE : (k + 1) * WIDE]


def call(kernel, outs, scratch, limit, *args):
    return pl.pallas_call(
        kernel,
        out_shape=outs,
        in_specs=[VMEM] * len(args),
        out_specs=[VMEM] * len(outs),
        scratch_shapes=scratch,
        compiler_params=pltpu.CompilerParams(vmem_limit_bytes=limit * 1024 * 1024),
    )(*args)


def shape(dims, dtype):
    return jax.ShapeDtypeStruct(dims, dtype)


def exchange(value, axes):
    return lax.all_to_all(value, axes, split_axis=0, concat_axis=0)


def per_device(weights, momentum, gradients):
    new_momentum = MOMENTUM_DECAY * momentum + gradients
    iterate = gradients + MOMENTUM_DECAY * new_momentum
    plain = iterate.astype(BF)

    near = exchange(jnp.stack([plain[0], plain[0], plain[1], plain[1]]), ("m", "y0"))
    far = swap(near, "c")
    partial, own_rows = call(
        gram_kernel,
        (shape((TILE, PACK), BF), shape((ROWS, D), BF)),
        [pltpu.VMEM((352, D), BF)],
        16,
        near, far,
    )
    pieces = exchange(partial.reshape(16, GROWS, PACK), ("z", "x"))
    gram_rows = jnp.sum(pieces.astype(F32), axis=0).astype(BF)

    def whole(spread):
        part = exchange(spread, ("y0", "z", "x")).reshape(D // 2, PACK)
        return part, swap(part, "c")

    own, away = whole(jnp.broadcast_to(gram_rows[None], (32, GROWS, PACK)))
    spread, x1 = call(
        first_kernel,
        (shape((32, GROWS, PACK), BF), shape((ROWS, D), F32)),
        [
            pltpu.VMEM((D, D), BF),
            pltpu.VMEM((GROWS + ROWS, D), BF),
            pltpu.VMEM((GROWS + ROWS, D), BF),
            pltpu.VMEM((GROWS + ROWS, D), F32),
            pltpu.VMEM((GROWS, D), F32),
            pltpu.VMEM((GROWS, D), F32),
            pltpu.VMEM((GROWS, D), BF),
        ],
        32,
        own, away, own_rows,
    )
    own, away = whole(spread)
    (x3,) = call(
        second_kernel,
        (shape((8, ROWS, WIDE), BF),),
        [pltpu.VMEM((D, D), BF), pltpu.VMEM((2, ROWS, D), BF), pltpu.VMEM((5, ROWS, D), F32)],
        32,
        own, away, x1,
    )

    back = exchange(x3, ("c", "m", "y0")).reshape(2, 2, 2, ROWS, WIDE)
    both = back.transpose(1, 0, 2, 3, 4).reshape(2, 352, WIDE)

    update = STEP_SCALE * math.sqrt(max(FF, D)) * both.astype(F32)
    new_weights = weights * (1.0 - LEARN_RATE * WEIGHT_DECAY) - LEARN_RATE * update
    return (new_weights, new_momentum, update)


def solution(mesh):
    fine = Mesh(mesh.devices.reshape(4, 4, 2, 2, 2), ("z", "x", "m", "y0", "c"))
    spec = P(None, ("z", "x"), ("m", "y0", "c"))
    return jax.shard_map(
        per_device, mesh=fine, in_specs=(spec, spec, spec), out_specs=(spec, spec, spec), check_vma=False
    )
```

time: 195 us -> 173 us (0.89)
  Pallas kernels: 48.6 us -> 31 us
  local copies, waits for them, and re-layouts: 4.89 us -> 1.22 us
    pallas_call x3, Pallas kernels: 48.6 us -> 31 us  [call(): pl.pallas_call(kernel, out_shape=outs, in_specs=[VMEM] * len(args), out_s...]
    unnamed x14 -> x2, local copies, waits for them, and re-layouts: 3.73 us -> 0.06 us
where the time goes in v4:
time: 173 us
  blocking collectives  119 us (69%)
  Pallas kernels  31 us (18%)
  waiting for transfers between devices  10.1 us (6%)
  starting transfers between devices  7 us (4%)
  other arithmetic  3.64 us (2%)
    all_to_all x5, blocking collectives, exchange(): return lax.all_to_all(value, axes, split_axis=0, concat_axis=0)  119 us
    pallas_call x3, Pallas kernels, call(): pl.pallas_call(kernel, out_shape=outs, in_specs=[VMEM] * len(args), out_s...  31 us
    ppermute x3, waiting for transfers between devices, swap(): return lax.ppermute(value, axis, [(0, 1), (1, 0)])  10.1 us
    ppermute x3, starting transfers between devices, swap(): return lax.ppermute(value, axis, [(0, 1), (1, 0)])  7 us
  transfers between devices with their start and end apart: 3, of which 3 were waited for; matrix products, arithmetic and copies ran while one was open for 0% of the time, Pallas kernels for 0%

profile of v4, /device:TPU:1, one launch (start us, length us, event | category | flops | bytes accessed | tf_op | source)
XLA Modules:
  0.0 172.5 jit_solution(15203349931442295998)
XLA Ops:
  0.6 2.3 %add_convert_fusion = (bf16[2,352,256]{2,1,0:T(8,128)(2,1)S(1)}, f32[2,352,256]{2,1,0:T(8,128)}) fusion(f32[2,352,256]{2,1,0:T(8,128)} %param.5, f32[2,352,256]{2,1,0:T(8,128)} %param.4), kind=kLoop, calls=%fused_computation.4 | loop fusion | flops 901120 | bytes 2523136 | tf_op jit(solution)/shard_map/convert_element_type | solution.py:214
  3.0 0.1 pad_maximum_fusion
  3.1 15.2 %all_to_all.25.near = bf16[4,352,256]{2,1,0:T(8,128)(2,1)S(1)} all-to-all(bf16[4,352,256]{2,1,0:T(8,128)(2,1)S(1)} %pad_maximum_fusion), channel_id=1, replica_groups=mesh['z'=4,'x'=4,'m'=2,'y0'=2,'c'=2] {'m','y0'}, dimensions={0} | all-to-all | bytes 1441792 | tf_op jit(solution)/shard_map/all_to_all | solution.py:208
  18.3 2.1 %collective-permute-start = (bf16[4,352,256]{2,1,0:T(8,128)(2,1)S(1)}, bf16[4,352,256]{2,1,0:T(8,128)(2,1)S(1)}, u32[]{:S(2)}, u32[]{:S(2)}) collective-permute-start(bf16[4,352,256]{2,1,0:T(8,128)(2,1)S(1)} %all_to_all.25.near), channel_id=1, source_target_pairs={{0,1},{1,0},{2,3},{3,2},{4,5},{5,4},{6,7},{7,6},{8,9},{9,8},{10,11... | collective-permute-start | bytes 2162696 | tf_op jit(solution)/shard_map/ppermute | solution.py:45
  20.4 1.8 %collective-permute-done.far = bf16[4,352,256]{2,1,0:T(8,128)(2,1)S(1)} collective-permute-done((bf16[4,352,256]{2,1,0:T(8,128)(2,1)S(1)}, bf16[4,352,256]{2,1,0:T(8,128)(2,1)S(1)}, u32[]{:S(2)}, u32[]{:S(2)}) %collective-permute-start) | collective-permute-done | bytes 720928 | tf_op jit(solution)/shard_map/ppermute | solution.py:45
  22.2 1.0 shard_map.58
  23.3 25.4 %all_to_all.26 = bf16[16,32,1152]{2,1,0:T(8,128)(2,1)S(1)} all-to-all(bf16[16,32,1152]{2,1,0:T(8,128)(2,1)S(1)} %bitcast.16), channel_id=1, replica_groups=mesh['z'=4,'x'=4,'m'=2,'y0'=2,'c'=2] {'z','x'}, dimensions={0} | all-to-all | bytes 2359296 | tf_op jit(solution)/shard_map/all_to_all | solution.py:208
  48.7 0.2 reduce_sum.12
  48.9 0.2 broadcast_in_dim.2
  49.1 33.1 %all_to_all.27 = bf16[32,32,1152]{2,1,0:T(8,128)(2,1)S(1)} all-to-all(bf16[32,32,1152]{2,1,0:T(8,128)(2,1)S(1)} %broadcast_in_dim.2), channel_id=1, replica_groups=mesh['z'=4,'x'=4,'m'=2,'y0'=2,'c'=2] {'y0','z','x'}, dimensions={0} | all-to-all | bytes 4718592 | tf_op jit(solution)/shard_map/all_to_all | solution.py:208
  82.2 2.6 %collective-permute-start.1 = (bf16[1024,1152]{1,0:T(8,128)(2,1)S(1)}, bf16[1024,1152]{1,0:T(8,128)(2,1)S(1)}, u32[]{:S(2)}, u32[]{:S(2)}) collective-permute-start(bf16[1024,1152]{1,0:T(8,128)(2,1)S(1)} %bitcast.12), channel_id=1, source_target_pairs={{0,1},{1,0},{2,3},{3,2},{4,5},{5,4},{6,7},{7,6},{8,9},{9,8},{10,11... | collective-permute-start | bytes 7077896 | tf_op jit(solution)/shard_map/ppermute | solution.py:45
  84.9 4.2 %collective-permute-done.1.other = bf16[1024,1152]{1,0:T(8,128)(2,1)S(1)} collective-permute-done((bf16[1024,1152]{1,0:T(8,128)(2,1)S(1)}, bf16[1024,1152]{1,0:T(8,128)(2,1)S(1)}, u32[]{:S(2)}, u32[]{:S(2)}) %collective-permute-start.1) | collective-permute-done | bytes 2359328 | tf_op jit(solution)/shard_map/ppermute | solution.py:45
  89.0 8.0 %shard_map.59 = (bf16[32,32,1152]{2,1,0:T(8,128)(2,1)S(1)}, f32[88,2048]{1,0:T(8,128)S(1)}) custom-call(bf16[1024,1152]{1,0:T(8,128)(2,1)S(1)} %bitcast.13, bf16[1024,1152]{1,0:T(8,128)(2,1)S(1)} %collective-permute-done.1.other, bf16[88,2048]{1,0:T(8,128)(2,1)S(1)} %get-tuple-element.8.plain), custom_call_target="tpu_custom_call" | custom-call | tf_op jit(solution)/shard_map/pallas_call | solution.py:193
  97.0 33.7 %all_to_all.28 = bf16[32,32,1152]{2,1,0:T(8,128)(2,1)S(1)} all-to-all(bf16[32,32,1152]{2,1,0:T(8,128)(2,1)S(1)} %get-tuple-element.9), channel_id=1, replica_groups=mesh['z'=4,'x'=4,'m'=2,'y0'=2,'c'=2] {'y0','z','x'}, dimensions={0} | all-to-all | bytes 4718592 | tf_op jit(solution)/shard_map/all_to_all | solution.py:208
  130.7 2.3 %collective-permute-start.2 = (bf16[1024,1152]{1,0:T(8,128)(2,1)S(1)}, bf16[1024,1152]{1,0:T(8,128)(2,1)S(1)}, u32[]{:S(2)}, u32[]{:S(2)}) collective-permute-start(bf16[1024,1152]{1,0:T(8,128)(2,1)S(1)} %bitcast.14), channel_id=1, source_target_pairs={{0,1},{1,0},{2,3},{3,2},{4,5},{5,4},{6,7},{7,6},{8,9},{9,8},{10,11... | collective-permute-start | bytes 7077896 | tf_op jit(solution)/shard_map/ppermute | solution.py:45
  133.0 4.2 %collective-permute-done.2.other = bf16[1024,1152]{1,0:T(8,128)(2,1)S(1)} collective-permute-done((bf16[1024,1152]{1,0:T(8,128)(2,1)S(1)}, bf16[1024,1152]{1,0:T(8,128)(2,1)S(1)}, u32[]{:S(2)}, u32[]{:S(2)}) %collective-permute-start.2) | collective-permute-done | bytes 2359328 | tf_op jit(solution)/shard_map/ppermute | solution.py:45
  137.1 22.0 %shard_map.60 = bf16[8,88,256]{2,1,0:T(8,128)(2,1)S(1)} custom-call(bf16[1024,1152]{1,0:T(8,128)(2,1)S(1)} %bitcast.15, bf16[1024,1152]{1,0:T(8,128)(2,1)S(1)} %collective-permute-done.2.other, f32[88,2048]{1,0:T(8,128)S(1)} %get-tuple-element.10.x1), custom_call_target="tpu_custom_call" | custom-call | tf_op jit(solution)/shard_map/pallas_call | solution.py:193
  159.1 11.3 %all_to_all.29 = bf16[8,88,256]{2,1,0:T(8,128)(2,1)S(1)} all-to-all(bf16[8,88,256]{2,1,0:T(8,128)(2,1)S(1)} %shard_map.60), channel_id=1, replica_groups=mesh['z'=4,'x'=4,'m'=2,'y0'=2,'c'=2] {'c','m','y0'}, dimensions={0} | all-to-all | bytes 720896 | tf_op jit(solution)/shard_map/all_to_all | solution.py:208
  170.4 0.0 copy-start
  170.4 0.1 convert_multiply_fusion
  170.5 0.9 copy.7
  171.5 0.1 copy-done
  171.6 1.0 bitcast_subtract_fusion
  (2 shorter events, 0.1 us)
Async XLA Ops:
  18.3 3.9 %collective-permute-start = (bf16[4,352,256]{2,1,0:T(8,128)(2,1)S(1)}, bf16[4,352,256]{2,1,0:T(8,128)(2,1)S(1)}, u32[]{:S(2)}, u32[]{:S(2)}) collective-permute-start(bf16[4,352,256]{2,1,0:T(8,128)(2,1)S(1)} %all_to_all.25.near), channel_id=1, source_target_pairs={{0,1},{1,0},{2,3},{3,2},{4,5},{5,4},{6,7},{7,6},{8,9},{9,8},{10,11... | collective-permute-start | bytes 2162696 | tf_op jit(solution)/shard_map/ppermute | solution.py:45
  82.2 6.8 %collective-permute-start.1 = (bf16[1024,1152]{1,0:T(8,128)(2,1)S(1)}, bf16[1024,1152]{1,0:T(8,128)(2,1)S(1)}, u32[]{:S(2)}, u32[]{:S(2)}) collective-permute-start(bf16[1024,1152]{1,0:T(8,128)(2,1)S(1)} %bitcast.12), channel_id=1, source_target_pairs={{0,1},{1,0},{2,3},{3,2},{4,5},{5,4},{6,7},{7,6},{8,9},{9,8},{10,11... | collective-permute-start | bytes 7077896 | tf_op jit(solution)/shard_map/ppermute | solution.py:45
  130.7 6.4 %collective-permute-start.2 = (bf16[1024,1152]{1,0:T(8,128)(2,1)S(1)}, bf16[1024,1152]{1,0:T(8,128)(2,1)S(1)}, u32[]{:S(2)}, u32[]{:S(2)}) collective-permute-start(bf16[1024,1152]{1,0:T(8,128)(2,1)S(1)} %bitcast.14), channel_id=1, source_target_pairs={{0,1},{1,0},{2,3},{3,2},{4,5},{5,4},{6,7},{7,6},{8,9},{9,8},{10,11... | collective-permute-start | bytes 7077896 | tf_op jit(solution)/shard_map/ppermute | solution.py:45
  170.4 1.2 copy-start

commit v5 on v4

--- a/solution.py
+++ b/solution.py
@@ -144,49 +144,73 @@
     lax.fori_loop(0, 32, spread, 0)
 
 
-X1, X2, T, Y, Z = range(5)
+X2, T, Y, Z = range(4)
 
 
 def second_kernel(own, other, x1, out, full, left, buf):
     core = lax.axis_index("c")
     unpack(full, own, other)
-    buf[X1] = x1[...]
-    buf[T] = jnp.zeros((ROWS, D), F32)
-    buf[Y] = jnp.zeros((ROWS, D), F32)
     left[0] = x1[...].astype(BF)
-
-    def product(i, carry):
-        keep = jnp.logical_or(i == 2, i == 7)
-        less = (i == 0) | (i == 3) | (i == 5) | (i == 8) | (i == 10)
-        scale = jnp.where(jnp.logical_or(keep, less), 1.0, A3)
-        scale_base = jnp.where(keep, 0.0, jnp.where(less, -SHIFT, REST))
-        scale_y = jnp.where(jnp.logical_or(keep, less), 0.0, -A3 * SHIFT)
-        base = jnp.where(i < 2, X1, T)
-        into = jnp.where(less, Y, jnp.where(i == 1, X2, jnp.where(i == 6, Z, T)))
-        src = lax.rem(i, 2)
-        for n in range(D // TILE):
-            sl = slice(n * TILE, (n + 1) * TILE)
-            value = scale * dot(left[src], full[:, sl])
-            value = value + scale_base * buf[base, :, sl] + scale_y * buf[Y, :, sl]
-            buf[into, :, sl] = value
+    turn = [0]
+
+    def times(finish):
+        src = turn[0]
+        turn[0] = 1 - src
+
+        def body(n, sl):
+            value = finish(sl, dot(left[src], full[:, sl]))
             left[1 - src, :, sl] = value.astype(BF)
 
-        @pl.when(i == 6)
-        def _():
-            value = buf[Z] - SHIFT * buf[X2]
-            buf[Z] = value
-            left[1 - src] = value.astype(BF)
-
-        return carry
-
-    lax.fori_loop(0, 11, product, 0)
-    for n in range(D // TILE):
-        sl = slice(n * TILE, (n + 1) * TILE)
-        value = dot(left[1], full[:, sl]) - SHIFT * buf[Y, :, sl]
+        columns(body)
+
+    def first_less(sl, value):
+        value = value - SHIFT * x1[:, sl]
+        buf[Y, :, sl] = value
+        return value
+
+    def first_close(sl, value):
+        value = REST * x1[:, sl] + A3 * (value - SHIFT * buf[Y, :, sl])
+        buf[X2, :, sl] = value
+        return value
+
+    def keep(sl, value):
+        buf[T, :, sl] = value
+        return value
+
+    def less(sl, value):
+        value = value - SHIFT * buf[T, :, sl]
+        buf[Y, :, sl] = value
+        return value
+
+    def close(sl, value):
+        value = REST * buf[T, :, sl] + A3 * (value - SHIFT * buf[Y, :, sl])
+        buf[T, :, sl] = value
+        return value
+
+    def middle(sl, value):
+        value = REST * buf[T, :, sl] + A3 * (value - SHIFT * buf[Y, :, sl])
+        value = value - SHIFT * buf[X2, :, sl]
+        buf[Z, :, sl] = value
+        return value
+
+    for finish in (first_less, first_close):
+        times(finish)
+    for finish in (keep, less, close, less, middle):
+        times(finish)
+    for finish in (keep, less, close, less):
+        times(finish)
+
+    def last(n, sl):
+        value = dot(left[turn[0]], full[:, sl]) - SHIFT * buf[Y, :, sl]
         value = REST * buf[T, :, sl] + A3 * value - SHIFT * buf[Z, :, sl]
         value = (REST * buf[X2, :, sl] + A3 * value).astype(BF)
         for k in range(2):
-            out[lax.rem(2 * n + k + core * 4, 8)] = value[:, k * WIDE : (k + 1) * WIDE]
+            block = 2 * n + k
+            there = lax.rem(block // 4 + core, 2)
+            y = block % 4
+            out[(y // 2) * 4 + there * 2 + y % 2] = value[:, k * WIDE : (k + 1) * WIDE]
+
+    columns(last)
 
 
 def call(kernel, outs, scratch, limit, *args):
@@ -249,13 +273,12 @@
     (x3,) = call(
         second_kernel,
         (shape((8, ROWS, WIDE), BF),),
-        [pltpu.VMEM((D, D), BF), pltpu.VMEM((2, ROWS, D), BF), pltpu.VMEM((5, ROWS, D), F32)],
+        [pltpu.VMEM((D, D), BF), pltpu.VMEM((2, ROWS, D), BF), pltpu.VMEM((4, ROWS, D), F32)],
         32,
         own, away, x1,
     )
 
-    back = exchange(x3, ("c", "m", "y0")).reshape(2, 2, 2, ROWS, WIDE)
-    both = back.transpose(1, 0, 2, 3, 4).reshape(2, 352, WIDE)
+    both = exchange(x3, ("m", "c", "y0")).reshape(2, 352, WIDE)
 
     update = STEP_SCALE * math.sqrt(max(FF, D)) * both.astype(F32)
     new_weights = weights * (1.0 - LEARN_RATE * WEIGHT_DECAY) - LEARN_RATE * update

time: 173 us -> 165 us (0.954)
  Pallas kernels: 31 us -> 23.7 us
    pallas_call x3, Pallas kernels: 31 us -> 23.7 us  [call(): pl.pallas_call(kernel, out_shape=outs, in_specs=[VMEM] * len(args), out_s...]
where the time goes in v5:
time: 165 us
  blocking collectives  119 us (72%)
  Pallas kernels  23.7 us (14%)
  waiting for transfers between devices  10.1 us (6%)
  starting transfers between devices  7 us (4%)
  other arithmetic  4.5 us (3%)
    all_to_all x5, blocking collectives, exchange(): return lax.all_to_all(value, axes, split_axis=0, concat_axis=0)  119 us
    pallas_call x3, Pallas kernels, call(): pl.pallas_call(kernel, out_shape=outs, in_specs=[VMEM] * len(args), out_s...  23.7 us
    ppermute x3, waiting for transfers between devices, swap(): return lax.ppermute(value, axis, [(0, 1), (1, 0)])  10.1 us
    ppermute x3, starting transfers between devices, swap(): return lax.ppermute(value, axis, [(0, 1), (1, 0)])  7 us
  transfers between devices with their start and end apart: 3, of which 3 were waited for; matrix products, arithmetic and copies ran while one was open for 0% of the time, Pallas kernels for 0%

profile of v5, /device:TPU:1, one launch (start us, length us, event | category | flops | bytes accessed | tf_op | source)
XLA Modules:
  0.0 165.1 jit_solution(530743112521527595)
XLA Ops:
  0.6 2.3 %add_convert_fusion = (bf16[2,352,256]{2,1,0:T(8,128)(2,1)S(1)}, f32[2,352,256]{2,1,0:T(8,128)}) fusion(f32[2,352,256]{2,1,0:T(8,128)} %param.5, f32[2,352,256]{2,1,0:T(8,128)} %param.4), kind=kLoop, calls=%fused_computation.4 | loop fusion | flops 901120 | bytes 2523136 | tf_op jit(solution)/shard_map/convert_element_type | solution.py:238
  3.0 0.1 pad_maximum_fusion
  3.1 15.2 %all_to_all.25.near = bf16[4,352,256]{2,1,0:T(8,128)(2,1)S(1)} all-to-all(bf16[4,352,256]{2,1,0:T(8,128)(2,1)S(1)} %pad_maximum_fusion), channel_id=1, replica_groups=mesh['z'=4,'x'=4,'m'=2,'y0'=2,'c'=2] {'m','y0'}, dimensions={0} | all-to-all | bytes 1441792 | tf_op jit(solution)/shard_map/all_to_all | solution.py:232
  18.3 2.1 %collective-permute-start = (bf16[4,352,256]{2,1,0:T(8,128)(2,1)S(1)}, bf16[4,352,256]{2,1,0:T(8,128)(2,1)S(1)}, u32[]{:S(2)}, u32[]{:S(2)}) collective-permute-start(bf16[4,352,256]{2,1,0:T(8,128)(2,1)S(1)} %all_to_all.25.near), channel_id=1, source_target_pairs={{0,1},{1,0},{2,3},{3,2},{4,5},{5,4},{6,7},{7,6},{8,9},{9,8},{10,11... | collective-permute-start | bytes 2162696 | tf_op jit(solution)/shard_map/ppermute | solution.py:45
  20.4 1.8 %collective-permute-done.far = bf16[4,352,256]{2,1,0:T(8,128)(2,1)S(1)} collective-permute-done((bf16[4,352,256]{2,1,0:T(8,128)(2,1)S(1)}, bf16[4,352,256]{2,1,0:T(8,128)(2,1)S(1)}, u32[]{:S(2)}, u32[]{:S(2)}) %collective-permute-start) | collective-permute-done | bytes 720928 | tf_op jit(solution)/shard_map/ppermute | solution.py:45
  22.2 1.0 shard_map.58
  23.3 25.4 %all_to_all.26 = bf16[16,32,1152]{2,1,0:T(8,128)(2,1)S(1)} all-to-all(bf16[16,32,1152]{2,1,0:T(8,128)(2,1)S(1)} %bitcast.11), channel_id=1, replica_groups=mesh['z'=4,'x'=4,'m'=2,'y0'=2,'c'=2] {'z','x'}, dimensions={0} | all-to-all | bytes 2359296 | tf_op jit(solution)/shard_map/all_to_all | solution.py:232
  48.7 0.2 reduce_sum.12
  48.9 0.2 broadcast_in_dim.2
  49.1 33.1 %all_to_all.27 = bf16[32,32,1152]{2,1,0:T(8,128)(2,1)S(1)} all-to-all(bf16[32,32,1152]{2,1,0:T(8,128)(2,1)S(1)} %broadcast_in_dim.2), channel_id=1, replica_groups=mesh['z'=4,'x'=4,'m'=2,'y0'=2,'c'=2] {'y0','z','x'}, dimensions={0} | all-to-all | bytes 4718592 | tf_op jit(solution)/shard_map/all_to_all | solution.py:232
  82.2 2.6 %collective-permute-start.1 = (bf16[1024,1152]{1,0:T(8,128)(2,1)S(1)}, bf16[1024,1152]{1,0:T(8,128)(2,1)S(1)}, u32[]{:S(2)}, u32[]{:S(2)}) collective-permute-start(bf16[1024,1152]{1,0:T(8,128)(2,1)S(1)} %bitcast.7), channel_id=1, source_target_pairs={{0,1},{1,0},{2,3},{3,2},{4,5},{5,4},{6,7},{7,6},{8,9},{9,8},{10,11... | collective-permute-start | bytes 7077896 | tf_op jit(solution)/shard_map/ppermute | solution.py:45
  84.9 4.2 %collective-permute-done.1.other = bf16[1024,1152]{1,0:T(8,128)(2,1)S(1)} collective-permute-done((bf16[1024,1152]{1,0:T(8,128)(2,1)S(1)}, bf16[1024,1152]{1,0:T(8,128)(2,1)S(1)}, u32[]{:S(2)}, u32[]{:S(2)}) %collective-permute-start.1) | collective-permute-done | bytes 2359328 | tf_op jit(solution)/shard_map/ppermute | solution.py:45
  89.0 8.0 %shard_map.59 = (bf16[32,32,1152]{2,1,0:T(8,128)(2,1)S(1)}, f32[88,2048]{1,0:T(8,128)S(1)}) custom-call(bf16[1024,1152]{1,0:T(8,128)(2,1)S(1)} %bitcast.8, bf16[1024,1152]{1,0:T(8,128)(2,1)S(1)} %collective-permute-done.1.other, bf16[88,2048]{1,0:T(8,128)(2,1)S(1)} %get-tuple-element.8.plain), custom_call_target="tpu_custom_call" | custom-call | tf_op jit(solution)/shard_map/pallas_call | solution.py:217
  97.0 33.7 %all_to_all.28 = bf16[32,32,1152]{2,1,0:T(8,128)(2,1)S(1)} all-to-all(bf16[32,32,1152]{2,1,0:T(8,128)(2,1)S(1)} %get-tuple-element.9), channel_id=1, replica_groups=mesh['z'=4,'x'=4,'m'=2,'y0'=2,'c'=2] {'y0','z','x'}, dimensions={0} | all-to-all | bytes 4718592 | tf_op jit(solution)/shard_map/all_to_all | solution.py:232
  130.7 2.3 %collective-permute-start.2 = (bf16[1024,1152]{1,0:T(8,128)(2,1)S(1)}, bf16[1024,1152]{1,0:T(8,128)(2,1)S(1)}, u32[]{:S(2)}, u32[]{:S(2)}) collective-permute-start(bf16[1024,1152]{1,0:T(8,128)(2,1)S(1)} %bitcast.9), channel_id=1, source_target_pairs={{0,1},{1,0},{2,3},{3,2},{4,5},{5,4},{6,7},{7,6},{8,9},{9,8},{10,11... | collective-permute-start | bytes 7077896 | tf_op jit(solution)/shard_map/ppermute | solution.py:45
  133.0 4.2 %collective-permute-done.2.other = bf16[1024,1152]{1,0:T(8,128)(2,1)S(1)} collective-permute-done((bf16[1024,1152]{1,0:T(8,128)(2,1)S(1)}, bf16[1024,1152]{1,0:T(8,128)(2,1)S(1)}, u32[]{:S(2)}, u32[]{:S(2)}) %collective-permute-start.2) | collective-permute-done | bytes 2359328 | tf_op jit(solution)/shard_map/ppermute | solution.py:45
  137.1 14.7 %shard_map.60 = bf16[8,88,256]{2,1,0:T(8,128)(2,1)S(1)} custom-call(bf16[1024,1152]{1,0:T(8,128)(2,1)S(1)} %bitcast.10, bf16[1024,1152]{1,0:T(8,128)(2,1)S(1)} %collective-permute-done.2.other, f32[88,2048]{1,0:T(8,128)S(1)} %get-tuple-element.10.x1), custom_call_target="tpu_custom_call" | custom-call | tf_op jit(solution)/shard_map/pallas_call | solution.py:217
  151.8 0.0 copy-start
  151.9 11.3 %all_to_all.29 = bf16[8,88,256]{2,1,0:T(8,128)(2,1)S(1)} all-to-all(bf16[8,88,256]{2,1,0:T(8,128)(2,1)S(1)} %shard_map.60), channel_id=1, replica_groups=mesh['z'=4,'x'=4,'m'=2,'y0'=2,'c'=2] {'m','c','y0'}, dimensions={0} | all-to-all | bytes 720896 | tf_op jit(solution)/shard_map/all_to_all | solution.py:232
  163.1 1.0 convert_multiply_fusion
  164.1 0.0 copy-done
  164.1 1.0 bitcast_subtract_fusion
  (1 shorter events, 0.0 us)
Async XLA Ops:
  18.3 3.9 %collective-permute-start = (bf16[4,352,256]{2,1,0:T(8,128)(2,1)S(1)}, bf16[4,352,256]{2,1,0:T(8,128)(2,1)S(1)}, u32[]{:S(2)}, u32[]{:S(2)}) collective-permute-start(bf16[4,352,256]{2,1,0:T(8,128)(2,1)S(1)} %all_to_all.25.near), channel_id=1, source_target_pairs={{0,1},{1,0},{2,3},{3,2},{4,5},{5,4},{6,7},{7,6},{8,9},{9,8},{10,11... | collective-permute-start | bytes 2162696 | tf_op jit(solution)/shard_map/ppermute | solution.py:45
  82.2 6.8 %collective-permute-start.1 = (bf16[1024,1152]{1,0:T(8,128)(2,1)S(1)}, bf16[1024,1152]{1,0:T(8,128)(2,1)S(1)}, u32[]{:S(2)}, u32[]{:S(2)}) collective-permute-start(bf16[1024,1152]{1,0:T(8,128)(2,1)S(1)} %bitcast.7), channel_id=1, source_target_pairs={{0,1},{1,0},{2,3},{3,2},{4,5},{5,4},{6,7},{7,6},{8,9},{9,8},{10,11... | collective-permute-start | bytes 7077896 | tf_op jit(solution)/shard_map/ppermute | solution.py:45
  130.7 6.4 %collective-permute-start.2 = (bf16[1024,1152]{1,0:T(8,128)(2,1)S(1)}, bf16[1024,1152]{1,0:T(8,128)(2,1)S(1)}, u32[]{:S(2)}, u32[]{:S(2)}) collective-permute-start(bf16[1024,1152]{1,0:T(8,128)(2,1)S(1)} %bitcast.9), channel_id=1, source_target_pairs={{0,1},{1,0},{2,3},{3,2},{4,5},{5,4},{6,7},{7,6},{8,9},{9,8},{10,11... | collective-permute-start | bytes 7077896 | tf_op jit(solution)/shard_map/ppermute | solution.py:45
  151.8 12.3 %copy-start = (f32[2,352,256]{2,1,0:T(8,128)S(1)}, f32[2,352,256]{2,1,0:T(8,128)}, u32[]{:S(2)}) copy-start(f32[2,352,256]{2,1,0:T(8,128)} %param.3) | copy-start | bytes 2162692

commit v6 on v5

--- a/solution.py
+++ b/solution.py
@@ -98,50 +98,52 @@
             rows_out[...] = whole[k * ROWS : (k + 1) * ROWS, :]
 
 
-def first_kernel(own, other, plain, rows_out, x_out, full, l1, l2, u, hold, w, g1):
-    row = (lax.axis_index("y0") * 16 + lax.axis_index("z") * 4 + lax.axis_index("x")) * GROWS
+def first_kernel(own, other, q_out, full, scale_out):
     unpack(full, own, other)
     squares = square_sum((own, other))
     ratio = 1.0 / (NORM_SAFETY * jnp.sqrt(jnp.sqrt(squares / D)) + EPSILON)
+    scale_out[...] = jnp.broadcast_to(ratio, scale_out.shape)
     q = ratio * ratio
-    l1[:GROWS, :] = full[at(row, GROWS), :]
-    l1[GROWS:, :] = plain[...]
-
+
+    def panel(k, carry):
+        rows = at(k * BLK, BLK)
+        value = q * dot(full[rows, :], full[:, at(k * BLK, PACK, BLK)])
+        value = q * (A2 * own[rows, :].astype(F32) + A3 * value)
+        q_out[rows, :] = value.astype(BF)
+        return carry
+
+    lax.fori_loop(0, 8, panel, 0)
+
+
+def gram_step_kernel(own, other, gram, scale, g1_out, full, h, left):
+    unpack(full, own, other)
+    ratio = scale[:1, :1]
+    q = ratio * ratio
+
+    def panel(k, carry):
+        rows = at(k * BLK, BLK)
+
+        def one(n, sl):
+            value = dot(gram[rows, :], full[:, sl])
+            value = q * (A1 * gram[rows, sl].astype(F32) + value)
+            h[:, sl] = value
+            left[:, sl] = value.astype(BF)
+
+        columns(one)
+        window = at(k * BLK, PACK, BLK)
+        value = A1 * h[:, window] + dot(left[...], full[:, window])
+        g1_out[rows, :] = value.astype(BF)
+        return carry
+
+    lax.fori_loop(0, 8, panel, 0)
+
+
+def rows_step_kernel(plain, full, scale, out):
     def one(n, sl):
-        value = q * dot(l1[...], full[:, sl]) - SHIFT * l1[:, sl].astype(F32)
-        u[:, sl] = value
-        l2[:, sl] = value.astype(BF)
+        value = dot(plain[...], full[:, sl])
+        out[:, sl] = scale[:1, :1] * (A1 * plain[:, sl].astype(F32) + value)
 
     columns(one)
-
-    def two(n, sl):
-        value = q * dot(l2[...], full[:, sl])
-        mixed = REST * l1[:, sl].astype(F32) + A3 * (value - SHIFT * u[:, sl])
-        x_out[:, sl] = ratio * mixed[GROWS:]
-        hold[:, sl] = q * mixed[:GROWS]
-
-    columns(two)
-    l1[:GROWS, :] = hold[...].astype(BF)
-
-    def three(n, sl):
-        value = q * dot(l1[:GROWS, :], full[:, sl]) - SHIFT * hold[:, sl]
-        w[:, sl] = value
-        l2[:GROWS, sl] = value.astype(BF)
-
-    columns(three)
-
-    def four(n, sl):
-        value = q * dot(l2[:GROWS, :], full[:, sl])
-        g1[:, sl] = (REST * hold[:, sl] + A3 * (value - SHIFT * w[:, sl])).astype(BF)
-
-    columns(four)
-    packed = g1[:, at((row // BLK) * BLK, PACK, BLK)]
-
-    def spread(i, carry):
-        rows_out[i] = packed
-        return carry
-
-    lax.fori_loop(0, 32, spread, 0)
 
 
 X2, T, Y, Z = range(4)
@@ -249,27 +251,24 @@
     pieces = exchange(partial.reshape(16, GROWS, PACK), ("z", "x"))
     gram_rows = jnp.sum(pieces.astype(F32), axis=0).astype(BF)
 
-    def whole(spread):
-        part = exchange(spread, ("y0", "z", "x")).reshape(D // 2, PACK)
-        return part, swap(part, "c")
-
-    own, away = whole(jnp.broadcast_to(gram_rows[None], (32, GROWS, PACK)))
-    spread, x1 = call(
+    spread = jnp.broadcast_to(gram_rows[None], (32, GROWS, PACK))
+    own = exchange(spread, ("y0", "z", "x")).reshape(D // 2, PACK)
+    own_q, gram, scale = call(
         first_kernel,
-        (shape((32, GROWS, PACK), BF), shape((ROWS, D), F32)),
-        [
-            pltpu.VMEM((D, D), BF),
-            pltpu.VMEM((GROWS + ROWS, D), BF),
-            pltpu.VMEM((GROWS + ROWS, D), BF),
-            pltpu.VMEM((GROWS + ROWS, D), F32),
-            pltpu.VMEM((GROWS, D), F32),
-            pltpu.VMEM((GROWS, D), F32),
-            pltpu.VMEM((GROWS, D), BF),
-        ],
-        32,
-        own, away, own_rows,
-    )
-    own, away = whole(spread)
+        (shape((D // 2, PACK), BF), shape((D, D), BF), shape((8, BLK), F32)),
+        [],
+        24,
+        own, swap(own, "c"),
+    )
+    own, factor = call(
+        gram_step_kernel,
+        (shape((D // 2, PACK), BF), shape((D, D), BF)),
+        [pltpu.VMEM((BLK, D), F32), pltpu.VMEM((BLK, D), BF)],
+        24,
+        own_q, swap(own_q, "c"), gram, scale,
+    )
+    away = swap(own, "c")
+    (x1,) = call(rows_step_kernel, (shape((ROWS, D), F32),), [], 16, own_rows, factor, scale)
     (x3,) = call(
         second_kernel,
         (shape((8, ROWS, WIDE), BF),),

time: 165 us -> 156 us (0.945)
  blocking collectives: 119 us -> 85 us
  Pallas kernels: 23.7 us -> 46.3 us
  waiting for transfers between devices: 10.1 us -> 12.8 us
    all_to_all x5 -> x4, blocking collectives: 119 us -> 85 us  [exchange(): return lax.all_to_all(value, axes, split_axis=0, concat_axis=0)]
    pallas_call x3 -> x5, Pallas kernels: 23.7 us -> 46.3 us  [call(): pl.pallas_call(kernel, out_shape=outs, in_specs=[VMEM] * len(args), out_s...]
    ppermute x3 -> x4, waiting for transfers between devices: 10.1 us -> 12.8 us  [swap(): return lax.ppermute(value, axis, [(0, 1), (1, 0)])]
    ppermute x3 -> x4, starting transfers between devices: 7 us -> 5.82 us  [swap(): return lax.ppermute(value, axis, [(0, 1), (1, 0)])]
  transfers between devices with their start and end apart: 3 -> 4, of which waited for: 3 -> 4; matrix products, arithmetic and copies ran while one was open for 0% -> 0% of each run, Pallas kernels for 0% -> 1%
where the time goes in v6:
time: 156 us; the launch traced here: 155 us
  blocking collectives  85 us (54%)
  Pallas kernels  46.3 us (30%)
  waiting for transfers between devices  12.8 us (8%)
  starting transfers between devices  5.82 us (4%)
  other arithmetic  4.5 us (3%)
    all_to_all x4, blocking collectives, exchange(): return lax.all_to_all(value, axes, split_axis=0, concat_axis=0)  85 us
    pallas_call x5, Pallas kernels, call(): pl.pallas_call(kernel, out_shape=outs, in_specs=[VMEM] * len(args), out_s...  46.3 us
    ppermute x4, waiting for transfers between devices, swap(): return lax.ppermute(value, axis, [(0, 1), (1, 0)])  12.8 us
    ppermute x4, starting transfers between devices, swap(): return lax.ppermute(value, axis, [(0, 1), (1, 0)])  5.82 us
  transfers between devices with their start and end apart: 4, of which 4 were waited for; matrix products, arithmetic and copies ran while one was open for 0% of the time, Pallas kernels for 1%

profile of v6, /device:TPU:1, one launch (start us, length us, event | category | flops | bytes accessed | tf_op | source)
XLA Modules:
  0.0 155.4 jit_solution(8293253791196496600)
XLA Ops:
  0.6 2.3 %add_convert_fusion = (bf16[2,352,256]{2,1,0:T(8,128)(2,1)S(1)}, f32[2,352,256]{2,1,0:T(8,128)}) fusion(f32[2,352,256]{2,1,0:T(8,128)} %param.5, f32[2,352,256]{2,1,0:T(8,128)} %param.4), kind=kLoop, calls=%fused_computation.4 | loop fusion | flops 901120 | bytes 2523136 | tf_op jit(solution)/shard_map/convert_element_type | solution.py:240
  3.0 0.1 pad_maximum_fusion
  3.1 15.2 %all_to_all.20.near = bf16[4,352,256]{2,1,0:T(8,128)(2,1)S(1)} all-to-all(bf16[4,352,256]{2,1,0:T(8,128)(2,1)S(1)} %pad_maximum_fusion), channel_id=1, replica_groups=mesh['z'=4,'x'=4,'m'=2,'y0'=2,'c'=2] {'m','y0'}, dimensions={0} | all-to-all | bytes 1441792 | tf_op jit(solution)/shard_map/all_to_all | solution.py:234
  18.3 2.1 %collective-permute-start = (bf16[4,352,256]{2,1,0:T(8,128)(2,1)S(1)}, bf16[4,352,256]{2,1,0:T(8,128)(2,1)S(1)}, u32[]{:S(2)}, u32[]{:S(2)}) collective-permute-start(bf16[4,352,256]{2,1,0:T(8,128)(2,1)S(1)} %all_to_all.20.near), channel_id=1, source_target_pairs={{0,1},{1,0},{2,3},{3,2},{4,5},{5,4},{6,7},{7,6},{8,9},{9,8},{10,11... | collective-permute-start | bytes 2162696 | tf_op jit(solution)/shard_map/ppermute | solution.py:45
  20.4 1.8 %collective-permute-done.far = bf16[4,352,256]{2,1,0:T(8,128)(2,1)S(1)} collective-permute-done((bf16[4,352,256]{2,1,0:T(8,128)(2,1)S(1)}, bf16[4,352,256]{2,1,0:T(8,128)(2,1)S(1)}, u32[]{:S(2)}, u32[]{:S(2)}) %collective-permute-start) | collective-permute-done | bytes 720928 | tf_op jit(solution)/shard_map/ppermute | solution.py:45
  22.2 1.0 shard_map.58
  23.3 25.4 %all_to_all.21 = bf16[16,32,1152]{2,1,0:T(8,128)(2,1)S(1)} all-to-all(bf16[16,32,1152]{2,1,0:T(8,128)(2,1)S(1)} %bitcast.8), channel_id=1, replica_groups=mesh['z'=4,'x'=4,'m'=2,'y0'=2,'c'=2] {'z','x'}, dimensions={0} | all-to-all | bytes 2359296 | tf_op jit(solution)/shard_map/all_to_all | solution.py:234
  48.7 0.2 reduce_sum.12
  48.9 0.2 broadcast_in_dim.2
  49.1 33.1 %all_to_all.22 = bf16[32,32,1152]{2,1,0:T(8,128)(2,1)S(1)} all-to-all(bf16[32,32,1152]{2,1,0:T(8,128)(2,1)S(1)} %broadcast_in_dim.2), channel_id=1, replica_groups=mesh['z'=4,'x'=4,'m'=2,'y0'=2,'c'=2] {'y0','z','x'}, dimensions={0} | all-to-all | bytes 4718592 | tf_op jit(solution)/shard_map/all_to_all | solution.py:234
  82.2 2.6 %collective-permute-start.1 = (bf16[1024,1152]{1,0:T(8,128)(2,1)S(1)}, bf16[1024,1152]{1,0:T(8,128)(2,1)S(1)}, u32[]{:S(2)}, u32[]{:S(2)}) collective-permute-start(bf16[1024,1152]{1,0:T(8,128)(2,1)S(1)} %bitcast.6), channel_id=1, source_target_pairs={{0,1},{1,0},{2,3},{3,2},{4,5},{5,4},{6,7},{7,6},{8,9},{9,8},{10,11... | collective-permute-start | bytes 7077896 | tf_op jit(solution)/shard_map/ppermute | solution.py:45
  84.9 4.2 %collective-permute-done.1.other = bf16[1024,1152]{1,0:T(8,128)(2,1)S(1)} collective-permute-done((bf16[1024,1152]{1,0:T(8,128)(2,1)S(1)}, bf16[1024,1152]{1,0:T(8,128)(2,1)S(1)}, u32[]{:S(2)}, u32[]{:S(2)}) %collective-permute-start.1) | collective-permute-done | bytes 2359328 | tf_op jit(solution)/shard_map/ppermute | solution.py:45
  89.0 10.4 %shard_map.59 = (bf16[1024,1152]{1,0:T(8,128)(2,1)S(1)}, bf16[2048,2048]{1,0:T(8,128)(2,1)S(1)}, f32[8,128]{1,0:T(8,128)S(1)}) custom-call(bf16[1024,1152]{1,0:T(8,128)(2,1)S(1)} %bitcast.7, bf16[1024,1152]{1,0:T(8,128)(2,1)S(1)} %collective-permute-done.1.other), custom_call_target="tpu_custom_call" | custom-call | tf_op jit(solution)/shard_map/pallas_call | solution.py:219
  99.5 0.5 collective-permute-start.2
  99.9 4.2 %collective-permute-done.2.other = bf16[1024,1152]{1,0:T(8,128)(2,1)S(1)} collective-permute-done((bf16[1024,1152]{1,0:T(8,128)(2,1)S(1)}, bf16[1024,1152]{1,0:T(8,128)(2,1)S(1)}, u32[]{:S(2)}, u32[]{:S(2)}) %collective-permute-start.2) | collective-permute-done | bytes 2359328 | tf_op jit(solution)/shard_map/ppermute | solution.py:45
  104.1 18.7 %shard_map.60 = (bf16[1024,1152]{1,0:T(8,128)(2,1)S(1)}, bf16[2048,2048]{1,0:T(8,128)(2,1)S(1)}) custom-call(bf16[1024,1152]{1,0:T(8,128)(2,1)S(1)} %get-tuple-element.11.own, bf16[1024,1152]{1,0:T(8,128)(2,1)S(1)} %collective-permute-done.2.other, bf16[2048,2048]{1,0:T(8,128)(2,1)S(1)} %get-tuple-element.12.gram, f32[8,128]{1,0:T(8,128)S(1)} %get-tuple-element.13.scale), custom_call_target="tpu_custom_call" | custom-call | tf_op jit(solution)/shard_map/pallas_call | solution.py:219
  122.8 0.6 collective-permute-start.3
  123.4 1.5 shard_map.61.x1
  124.8 2.7 %collective-permute-done.3.other = bf16[1024,1152]{1,0:T(8,128)(2,1)S(1)} collective-permute-done((bf16[1024,1152]{1,0:T(8,128)(2,1)S(1)}, bf16[1024,1152]{1,0:T(8,128)(2,1)S(1)}, u32[]{:S(2)}, u32[]{:S(2)}) %collective-permute-start.3) | collective-permute-done | bytes 2359328 | tf_op jit(solution)/shard_map/ppermute | solution.py:45
  127.5 14.7 %shard_map.62 = bf16[8,88,256]{2,1,0:T(8,128)(2,1)S(1)} custom-call(bf16[1024,1152]{1,0:T(8,128)(2,1)S(1)} %get-tuple-element.14.own, bf16[1024,1152]{1,0:T(8,128)(2,1)S(1)} %collective-permute-done.3.other, f32[88,2048]{1,0:T(8,128)S(1)} %shard_map.61.x1), custom_call_target="tpu_custom_call" | custom-call | tf_op jit(solution)/shard_map/pallas_call | solution.py:219
  142.3 0.0 copy-start
  142.3 11.2 %all_to_all.23 = bf16[8,88,256]{2,1,0:T(8,128)(2,1)S(1)} all-to-all(bf16[8,88,256]{2,1,0:T(8,128)(2,1)S(1)} %shard_map.62), channel_id=1, replica_groups=mesh['z'=4,'x'=4,'m'=2,'y0'=2,'c'=2] {'m','c','y0'}, dimensions={0} | all-to-all | bytes 720896 | tf_op jit(solution)/shard_map/all_to_all | solution.py:234
  153.5 1.0 convert_multiply_fusion
  154.5 1.0 bitcast_subtract_fusion
  (2 shorter events, 0.0 us)
Async XLA Ops:
  18.3 3.9 %collective-permute-start = (bf16[4,352,256]{2,1,0:T(8,128)(2,1)S(1)}, bf16[4,352,256]{2,1,0:T(8,128)(2,1)S(1)}, u32[]{:S(2)}, u32[]{:S(2)}) collective-permute-start(bf16[4,352,256]{2,1,0:T(8,128)(2,1)S(1)} %all_to_all.20.near), channel_id=1, source_target_pairs={{0,1},{1,0},{2,3},{3,2},{4,5},{5,4},{6,7},{7,6},{8,9},{9,8},{10,11... | collective-permute-start | bytes 2162696 | tf_op jit(solution)/shard_map/ppermute | solution.py:45
  82.2 6.8 %collective-permute-start.1 = (bf16[1024,1152]{1,0:T(8,128)(2,1)S(1)}, bf16[1024,1152]{1,0:T(8,128)(2,1)S(1)}, u32[]{:S(2)}, u32[]{:S(2)}) collective-permute-start(bf16[1024,1152]{1,0:T(8,128)(2,1)S(1)} %bitcast.6), channel_id=1, source_target_pairs={{0,1},{1,0},{2,3},{3,2},{4,5},{5,4},{6,7},{7,6},{8,9},{9,8},{10,11... | collective-permute-start | bytes 7077896 | tf_op jit(solution)/shard_map/ppermute | solution.py:45
  99.5 4.6 %collective-permute-start.2 = (bf16[1024,1152]{1,0:T(8,128)(2,1)S(1)}, bf16[1024,1152]{1,0:T(8,128)(2,1)S(1)}, u32[]{:S(2)}, u32[]{:S(2)}) collective-permute-start(bf16[1024,1152]{1,0:T(8,128)(2,1)S(1)} %get-tuple-element.11.own), channel_id=1, source_target_pairs={{0,1},{1,0},{2,3},{3,2},{4,5},{5,4},{6,7},{7,6},{8,9},{9,8},{10,11... | collective-permute-start | bytes 7077896 | tf_op jit(solution)/shard_map/ppermute | solution.py:45
  122.8 4.8 %collective-permute-start.3 = (bf16[1024,1152]{1,0:T(8,128)(2,1)S(1)}, bf16[1024,1152]{1,0:T(8,128)(2,1)S(1)}, u32[]{:S(2)}, u32[]{:S(2)}) collective-permute-start(bf16[1024,1152]{1,0:T(8,128)(2,1)S(1)} %get-tuple-element.14.own), channel_id=1, source_target_pairs={{0,1},{1,0},{2,3},{3,2},{4,5},{5,4},{6,7},{7,6},{8,9},{9,8},{10,11... | collective-permute-start | bytes 7077896 | tf_op jit(solution)/shard_map/ppermute | solution.py:45
  142.3 12.2 %copy-start = (f32[2,352,256]{2,1,0:T(8,128)S(1)}, f32[2,352,256]{2,1,0:T(8,128)}, u32[]{:S(2)}) copy-start(f32[2,352,256]{2,1,0:T(8,128)} %param.3) | copy-start | bytes 2162692
